TPU v7x, 128 devices: a whole 4x4x4 slice. The times are simulated.
128 devices in a mesh: ep: 16 (over z, x), tp: 8 (over y, core).
Axes of the slice: x: 4, y: 4, z: 4, core: 2. Of those that a mesh axis runs over, the one named last changes fastest.
Arguments:
- mixer_input: bfloat16 [16384, 2048], P(('ep', 'tp')), may hold values from -6 to 6
- log_decay: float32 [16384, 8], P('ep', 'tp'), may hold values from -0.8 to 0
- mixer_gain: float32 [2048], replicated, may hold values from 0.1 to 1.9
- query_weight: bfloat16 [2048, 1024], P(None, 'tp'), may hold values from -0.125 to 0.125
- key_weight: bfloat16 [2048, 1024], P(None, 'tp'), may hold values from -0.125 to 0.125
- value_weight: bfloat16 [2048, 2048], P(None, 'tp'), may hold values from -0.125 to 0.125
- gate_weight: bfloat16 [2048, 2048], P(None, 'tp'), may hold values from -0.125 to 0.125
- head_gain: float32 [2048], P('tp'), may hold values from 0.1 to 1.9
- output_weight: bfloat16 [2048, 2048], P('tp'), may hold values from -0.125 to 0.125
- expert_input: bfloat16 [16384, 2048], P(('ep', 'tp')), may hold values from -6 to 6
- expert_gain: float32 [2048], replicated, may hold values from 0.1 to 1.9
- routes: int32 [16384, 2], P(('ep', 'tp')), may hold values from 0 to 127, as said below
- group_weight: float32 [16384], P(('ep', 'tp')), may hold values from 0.3 to 1
- pair_weight: float32 [16384, 2], P(('ep', 'tp')), may hold values from 0.2 to 1
- expert_gate: bfloat16 [128, 2048, 1024], P(('ep', 'tp')), may hold values from -0.125 to 0.125
- expert_up: bfloat16 [128, 2048, 1024], P(('ep', 'tp')), may hold values from -0.125 to 0.125
- expert_down: bfloat16 [128, 1024, 2048], P(('ep', 'tp')), may hold values from -0.1875 to 0.1875
Outputs:
- mixer_output: bfloat16 [16384, 2048], P(('ep', 'tp'))
- expert_output: bfloat16 [16384, 2048], P(('ep', 'tp'))
Inputs may be any that keep to these rules, and one draw needn't show every extreme that they name: `routes`: in the rows of one device each expert is named at most 3 times; one expert is named exactly 3 times in the rows of every device. A row names two different experts of the same group, a group being 32 consecutive expert numbers.
All inputs are finite; a program needn't handle non-finite values.
Results may differ from a plain program's by a relative error of at most 0.023.
Values may be sent and summed in bfloat16 or wider, within the bound.
No kernel may reach another device: no remote copies, remote signals or barrier semaphores. Data moves between devices by JAX's collectives and lax.ppermute only.
A program may use at most 128 MiB of HBM per device.

v0:
```python
import jax
import jax.numpy as jnp
from jax import lax
from jax.experimental import pallas as pl
from jax.experimental.pallas import tpu as pltpu
from jax.sharding import PartitionSpec as P


KEY_DIM = 128
VALUE_DIM = 256
CHUNK = 256
CAP = 3
EPSILON = 1e-05
THETA = 10000.0
BF = jnp.bfloat16
F32 = jnp.float32
VM = pl.BlockSpec(memory_space=pltpu.VMEM)
SM = pl.BlockSpec(memory_space=pltpu.SMEM)


HBM = pl.BlockSpec(memory_space=pltpu.HBM)


def run(kernel, outs, args, scalars=0, flops=0, scratch=(), vmem=24 << 20, hbm=()):
    nbytes = sum(a.size * a.dtype.itemsize for a in args) + sum(
        o.size * o.dtype.itemsize for o in jax.tree.leaves(outs)
    )
    return pl.pallas_call(
        kernel,
        out_shape=outs,
        in_specs=[SM if i < scalars else HBM if i in hbm else VM for i in range(len(args))],
        out_specs=jax.tree.map(lambda _: VM, outs),
        scratch_shapes=list(scratch),
        compiler_params=pltpu.CompilerParams(vmem_limit_bytes=vmem),
        cost_estimate=pl.CostEstimate(flops=flops, bytes_accessed=nbytes, transcendentals=0),
    )(*args)


def after(value, *earlier):
    return lax.optimization_barrier((value, *earlier))[0]


def shape(dims, dtype=BF):
    return jax.ShapeDtypeStruct(dims, dtype)


def dot(a, b, ca=1, cb=0):
    return lax.dot_general(a, b, (((ca,), (cb,)), ((), ())), preferred_element_type=F32)


def silu(v):
    return v * (1.0 / (1.0 + jnp.exp(-v)))


def normalised(x, gain):
    x = x.astype(F32)
    centred = x - jnp.mean(x, axis=-1, keepdims=True)
    spread = jnp.mean(centred * centred, axis=-1, keepdims=True)
    return centred * lax.rsqrt(spread + EPSILON) * gain


def fetch(sems, *pairs):
    copies = [pltpu.make_async_copy(a, b, sems.at[i]) for i, (a, b) in enumerate(pairs)]
    for copy in copies:
        copy.start()
    for copy in copies:
        copy.wait()


def norm_kernel(x_hbm, gain_hbm, o_ref, x_ref, gain_ref, sems):
    fetch(sems, (x_hbm, x_ref), (gain_hbm, gain_ref))
    o_ref[...] = normalised(x_ref[...], gain_ref[...]).astype(BF)


def dispatch_kernel(x_hbm, gain_hbm, routes_hbm, o_ref, x_ref, gain_ref, routes_ref, sems):
    fetch(sems, (x_hbm, x_ref), (gain_hbm, gain_ref), (routes_hbm, routes_ref))
    rows = normalised(x_ref[...], gain_ref[...]).astype(BF)
    tokens = rows.shape[0]
    experts = o_ref.shape[0] * o_ref.shape[2]
    ids = lax.broadcasted_iota(jnp.int32, (experts, tokens), 0)
    named = (ids == routes_ref[0:1, :]) | (ids == routes_ref[1:2, :])
    named = jnp.where(named, 1.0, 0.0)
    before = lax.broadcasted_iota(jnp.int32, (tokens, tokens), 0) < lax.broadcasted_iota(
        jnp.int32, (tokens, tokens), 1
    )
    rank = dot(named.astype(BF), jnp.where(before, 1.0, 0.0).astype(BF))
    for slot in range(CAP):
        pick = jnp.where(rank == float(slot), named, 0.0).astype(BF)
        o_ref[:, slot] = dot(pick, rows).astype(BF).reshape(
            o_ref.shape[0], o_ref.shape[2], o_ref.shape[3]
        )


def permute_kernel(perm_ref, x_ref, o_ref):
    o_ref[...] = dot(perm_ref[...], x_ref[...]).astype(BF)


def hidden_kernel(x_ref, gate_ref, up_ref, perm_ref, o_ref):
    x = x_ref[...]
    hidden = (silu(dot(x, gate_ref[...])) * dot(x, up_ref[...])).astype(BF)
    o_ref[...] = dot(perm_ref[...], hidden).astype(BF)


def down_kernel(h_ref, down_ref, o_ref):
    o_ref[...] = dot(h_ref[...], down_ref[...]).reshape(o_ref.shape).astype(BF)


def combine_kernel(rows_ref, routes_ref, group_ref, pair_ref, cols_ref, o_ref):
    tokens = routes_ref.shape[0]
    ids = cols_ref[0:1, :]
    slots = cols_ref[1:2, :].astype(F32)
    weight = group_ref[...] * pair_ref[...]
    first = routes_ref[:, 0:1] == ids
    second = routes_ref[:, 1:2] == ids
    named = jnp.where(first | second, 1.0, 0.0).astype(BF)
    before = lax.broadcasted_iota(jnp.int32, (tokens, tokens), 1) < lax.broadcasted_iota(
        jnp.int32, (tokens, tokens), 0
    )
    rank = dot(jnp.where(before, 1.0, 0.0).astype(BF), named)
    mix = jnp.where(first, weight[:, 0:1], 0.0) + jnp.where(second, weight[:, 1:2], 0.0)
    mix = jnp.where(rank == slots, mix, 0.0)
    high = mix.astype(BF)
    low = (mix - high.astype(F32)).astype(BF)
    rows = rows_ref[...].reshape(ids.shape[1], rows_ref.shape[2])
    o_ref[...] = (dot(high, rows) + dot(low, rows)).astype(BF)


def project_kernel(*refs):
    *blocks, wq, wk, wv, wg, o_ref, w_ref, lhs, sems = refs
    copies, lower = [], 0
    for i, part in enumerate((wq, wk, wv, wg)):
        there = w_ref.at[:, lower : lower + part.shape[1]]
        copies.append(pltpu.make_async_copy(part, there, sems.at[i]))
        lower += part.shape[1]
    for copy in copies:
        copy.start()
    for i, block in enumerate(blocks):
        lhs[pl.ds(i * block.shape[0], block.shape[0]), :] = block[...]
    for copy in copies:
        copy.wait()
    o_ref[...] = dot(lhs[...], w_ref[...]).astype(BF)


def split_total(total, like):
    high = total.astype(BF).astype(F32)
    mid = (total - high).astype(BF).astype(F32)
    low = total - high - mid
    row = lax.broadcasted_iota(jnp.int32, like, 0)
    return jnp.where(row == 0, high, jnp.where(row == 1, mid, low)).astype(BF)


def prefix_sums(rows):
    n = rows.shape[1]
    upper = lax.broadcasted_iota(jnp.int32, (n, n), 0) <= lax.broadcasted_iota(jnp.int32, (n, n), 1)
    return lax.dot_general(
        rows, jnp.where(upper, 1.0, 0.0), (((1,), (0,)), ((), ())),
        precision=lax.Precision.HIGHEST, preferred_element_type=F32,
    )


def mixer_kernel(
    src_ref, early_ref, b0_ref, b1_ref, w_ref, turn_ref, decay_ref,
    g_ref, state_ref, local_ref, scaled_ref, lhs, buf,
):
    rows = b0_ref.shape[0]
    lhs[0:rows, :] = b0_ref[...]
    lhs[rows : 2 * rows, :] = b1_ref[...]
    late = dot(lhs[...], w_ref[...]).astype(BF)
    early = early_ref.shape[0] // rows
    for i in range(early + 2):
        here = pl.ds(pl.multiple_of(src_ref[i] * rows, rows), rows)
        if i < early:
            buf[here, :] = early_ref[i * rows : (i + 1) * rows, :]
        else:
            buf[here, :] = late[(i - early) * rows : (i - early + 1) * rows, :]
    g_ref[...] = buf[:, 2 * KEY_DIM + VALUE_DIM :]

    sums = prefix_sums(decay_ref[...])
    columns = sums.T
    causal = lax.broadcasted_iota(jnp.int32, (CHUNK, CHUNK), 0) >= lax.broadcasted_iota(
        jnp.int32, (CHUNK, CHUNK), 1
    )
    first = lax.broadcasted_iota(jnp.int32, (CHUNK, KEY_DIM), 1) < KEY_DIM // 2
    state, base = None, jnp.zeros((1, 1), F32)
    for i in range(buf.shape[0] // CHUNK):
        here = slice(i * CHUNK, (i + 1) * CHUNK)
        turn = turn_ref[here, :]
        other = pltpu.roll(turn, KEY_DIM // 2, 1)
        cosine = jnp.where(first, turn, other)
        sine = jnp.where(first, -other, turn)

        def rotated(lower):
            part = buf[here, lower : lower + KEY_DIM].astype(F32)
            return (part * cosine + pltpu.roll(part, KEY_DIM // 2, 1) * sine).astype(BF)

        query, key = rotated(0), rotated(KEY_DIM)
        value = buf[here, 2 * KEY_DIM : 2 * KEY_DIM + VALUE_DIM]
        row, col = sums[i : i + 1, :], columns[:, i : i + 1]
        weight = jnp.where(causal, jnp.exp(jnp.minimum(col - row, 0.0)), 0.0)
        decayed = (dot(query, key, 1, 1) * weight).astype(BF)
        out = dot(decayed, value)
        wide = query.astype(F32)
        if state is not None:
            out = out + dot((wide * jnp.exp(col)).astype(BF), state.astype(BF))
        local_ref[here, :] = out
        scaled_ref[here, :] = (wide * jnp.exp(col + base)).astype(BF)
        end = row[:, CHUNK - 1 : CHUNK]
        kept = (key.astype(F32) * jnp.exp(end - col)).astype(BF)
        update = dot(kept, value, 0, 0)
        state = update if state is None else state * jnp.exp(end) + update
        base = base + end
    state_ref[0:KEY_DIM, :] = state.astype(BF)
    state_ref[KEY_DIM:, :] = split_total(base, (8, VALUE_DIM))


def read_payload(ref):
    tail = ref[KEY_DIM:, :].astype(F32)
    return ref[0:KEY_DIM, :].astype(F32), tail[0:1] + tail[1:2] + tail[2:3]


def before_me(pos, parts):
    state, gone = 0.0, 0.0
    for j, (own, total) in enumerate(parts):
        between = 0.0
        for i, (_, other) in enumerate(parts):
            if i != j:
                inside = (pos[i] > pos[j]) & (pos[i] < pos[0])
                between = between + jnp.where(inside, other, 0.0)
        earlier = pos[j] < pos[0]
        state = state + jnp.where(earlier, own * jnp.exp(between), 0.0)
        gone = gone + jnp.where(earlier, total, 0.0)
    return state, gone


def x_kernel(pos_ref, p0, p1, p2, p3, prefix_ref, gone_ref, state_ref):
    pos = [pos_ref[i] for i in range(4)]
    parts = [read_payload(p) for p in (p0, p1, p2, p3)]
    state, gone = before_me(pos, parts)
    prefix_ref[...] = state
    gone_ref[...] = jnp.broadcast_to(jnp.exp(gone), gone_ref.shape)
    whole, total = 0.0, 0.0
    for j, (own, mine) in enumerate(parts):
        later = 0.0
        for i, (_, other) in enumerate(parts):
            if i != j:
                later = later + jnp.where(pos[i] > pos[j], other, 0.0)
        whole = whole + own * jnp.exp(later)
        total = total + mine
    state_ref[0:KEY_DIM, :] = whole.astype(BF)
    state_ref[KEY_DIM:, :] = split_total(total, (8, VALUE_DIM))


def gated_kernel(
    pos_ref, core_ref, p0, p1, p2, p3, prefix_ref, gone_ref, local_ref, scaled_ref, gate_ref,
    gain_ref, own_ref, twin_ref, buf,
):
    pos = [pos_ref[i] for i in range(4)]
    parts = [read_payload(p) for p in (p0, p1, p2, p3)]
    state, _ = before_me(pos, parts)
    incoming = (prefix_ref[...] + gone_ref[0:1, :] * state).astype(BF)
    retained = local_ref[...] + dot(scaled_ref[...], incoming)
    heads = normalised(retained, gain_ref[...])
    buf[...] = (silu(gate_ref[...].astype(F32)) * heads).astype(BF)
    core = core_ref[0]
    rows = own_ref.shape[0] // 4
    for y in range(4):
        there = slice(y * rows, (y + 1) * rows)
        own_ref[there, :] = buf[pl.ds(pl.multiple_of((2 * y + core) * rows, rows), rows), :]
        twin_ref[there, :] = buf[pl.ds(pl.multiple_of((2 * y + 1 - core) * rows, rows), rows), :]


def output_kernel(y_ref, own_ref, twin_ref, wo_ref, wt_ref, o0, o1, o2, o3, lhs, lht):
    rows = o0.shape[0]
    for k in range(4):
        here = slice(k * rows, (k + 1) * rows)
        there = pl.ds(pl.multiple_of(y_ref[k] * rows, rows), rows)
        lhs[here, :] = own_ref[there, :]
        lht[here, :] = twin_ref[there, :]
    out = (dot(lhs[...], wo_ref[...]) + dot(lht[...], wt_ref[...])).astype(BF)
    for k, ref in enumerate((o0, o1, o2, o3)):
        ref[...] = out[k * rows : (k + 1) * rows, :]


def sum_kernel(a, b, c, d, o_ref):
    o_ref[...] = (
        a[...].astype(F32) + b[...].astype(F32) + c[...].astype(F32) + d[...].astype(F32)
    ).astype(BF)


def core_swap(x):
    return lax.ppermute(x, "tp", [(t, t ^ 1) for t in range(8)])


def y_shift(x, k):
    return lax.ppermute(x, "tp", [(t, ((t // 2 + k) % 4) * 2 + t % 2) for t in range(8)])


def x_shift(x, k):
    return lax.ppermute(x, "ep", [(e, (e // 4) * 4 + (e + k) % 4) for e in range(16)])


def z_shift(x, k):
    return lax.ppermute(x, "ep", [(e, (e + 4 * k) % 16) for e in range(16)])


def exchange(x, axis):
    return lax.all_to_all(x, axis, split_axis=0, concat_axis=0, tiled=True)


def rotation(seg_rows):
    half = KEY_DIM // 2
    position = (lax.axis_index("ep") * seg_rows + jnp.arange(seg_rows, dtype=jnp.int32)).astype(F32)
    frequency = THETA ** (-jnp.arange(half, dtype=F32) / half)
    angles = position[:, None] * frequency[None, :]
    return jnp.concatenate([jnp.cos(angles), jnp.sin(angles)], axis=1)


def local(
    mixer_input,
    log_decay,
    mixer_gain,
    query_weight,
    key_weight,
    value_weight,
    gate_weight,
    head_gain,
    output_weight,
    expert_input,
    expert_gain,
    routes,
    group_weight,
    pair_weight,
    expert_gate,
    expert_up,
    expert_down,
):
    rows, width = mixer_input.shape
    seg_rows = log_decay.shape[0]
    ep, tp = lax.axis_index("ep"), lax.axis_index("tp")
    y, core = tp // 2, tp % 2
    n_ep, n_tp = lax.axis_size("ep"), lax.axis_size("tp")
    slots = n_ep * n_tp * CAP

    sems = lambda n: pltpu.SemaphoreType.DMA((n,))
    normed = run(
        norm_kernel,
        shape((rows, width)),
        (mixer_input, mixer_gain[None]),
        hbm=(0, 1),
        vmem=60 << 20,
        scratch=(pltpu.VMEM((rows, width), BF), pltpu.VMEM((1, width), F32), sems(2)),
    )
    from_below = y_shift(normed, 1)
    from_above = y_shift(normed, -1)
    from_far = y_shift(normed, 2)
    twin = core_swap(normed)

    outgoing = run(
        dispatch_kernel,
        shape((n_ep, CAP, n_tp, width)),
        (after(expert_input, normed), expert_gain[None], routes.T),
        flops=2 * slots * rows * width,
        hbm=(0, 1, 2),
        vmem=60 << 20,
        scratch=(
            pltpu.VMEM((rows, width), BF),
            pltpu.VMEM((1, width), F32),
            pltpu.VMEM((2, rows), jnp.int32),
            sems(3),
        ),
    )
    staged = exchange(outgoing, "ep")

    twin_out = core_swap(output_weight)
    weights = (query_weight, key_weight, value_weight, gate_weight)
    cols = sum(w.shape[1] for w in weights)
    turn = rotation(seg_rows)
    decay = jnp.pad(log_decay.reshape(-1, CHUNK), ((0, 8 - seg_rows // CHUNK), (0, 0)))

    below_twin, above_twin = core_swap(from_below), core_swap(from_above)
    early, joined = run(
        project_kernel,
        (shape((6 * rows, cols)), shape((width, cols))),
        (normed, twin, from_below, below_twin, from_above, above_twin, *weights),
        flops=2 * 6 * rows * width * cols,
        hbm=(6, 7, 8, 9),
        scratch=(pltpu.VMEM((6 * rows, width), BF), sems(4)),
    )
    far_twin = core_swap(from_far)
    away = jnp.array([0, 0, 3, 3, 1, 1, 2, 2], jnp.int32)
    flip = jnp.array([0, 1] * 4, jnp.int32)
    source = ((y + away) % 4) * 2 + (core + flip) % 2
    gate, state, local_out, scaled = run(
        mixer_kernel,
        (
            shape((seg_rows, VALUE_DIM)),
            shape((KEY_DIM + 8, VALUE_DIM)),
            shape((seg_rows, VALUE_DIM), F32),
            shape((seg_rows, KEY_DIM)),
        ),
        (source, early, from_far, far_twin, joined, turn, decay),
        scalars=1,
        flops=2 * 2 * rows * width * cols,
        scratch=(pltpu.VMEM((2 * rows, width), BF), pltpu.VMEM((seg_rows, cols), BF)),
    )

    index = jnp.arange(slots, dtype=jnp.int32)
    deep = n_ep * CAP
    to_tp = ((index % deep) * n_tp + index // deep)[:, None] == index[None, :]
    source_row = (index // CAP % n_tp) * deep + index // (CAP * n_tp) * CAP + index % CAP
    to_source = source_row[:, None] == index[None, :]
    to_tp, to_source = to_tp.astype(BF), to_source.astype(BF)
    turned = run(
        permute_kernel,
        shape((slots, width)),
        (to_tp, after(staged, state).reshape(slots, width)),
        flops=2 * slots * slots * width,
    )
    tokens = exchange(turned.reshape(n_tp, deep, width), "tp").reshape(slots, width)

    shifts = jnp.array([0, -1, 1, 2], jnp.int32)
    x_pos = (ep % 4 + shifts + 4) % 4
    z_pos = (ep // 4 + shifts + 4) % 4
    payloads = (state, x_shift(state, 1), x_shift(state, -1), x_shift(state, 2))
    prefix, gone, plane = run(
        x_kernel,
        (
            shape((KEY_DIM, VALUE_DIM), F32),
            shape((8, VALUE_DIM), F32),
            shape((KEY_DIM + 8, VALUE_DIM)),
        ),
        (x_pos, *payloads),
        scalars=1,
    )
    planes = (plane, z_shift(plane, 1), z_shift(plane, -1), z_shift(plane, 2))
    own_gated, twin_gated = run(
        gated_kernel,
        (shape((4 * rows, VALUE_DIM)), shape((4 * rows, VALUE_DIM))),
        (z_pos, core.reshape(1), *planes, prefix, gone, local_out, scaled, gate, head_gain[None]),
        scalars=2,
        flops=2 * seg_rows * KEY_DIM * VALUE_DIM,
        scratch=(pltpu.VMEM((seg_rows, VALUE_DIM), BF),),
    )
    inner = expert_gate.shape[2]
    tile, wide = 256, 512
    params = pltpu.CompilerParams(
        vmem_limit_bytes=60 << 20, dimension_semantics=("arbitrary",)
    )
    expand = pl.pallas_call(
        hidden_kernel,
        grid=(inner // tile,),
        out_shape=shape((slots, inner)),
        in_specs=[
            pl.BlockSpec((slots, width), lambda f: (0, 0)),
            pl.BlockSpec((width, tile), lambda f: (0, f)),
            pl.BlockSpec((width, tile), lambda f: (0, f)),
            pl.BlockSpec((slots, slots), lambda f: (0, 0)),
        ],
        out_specs=pl.BlockSpec((slots, tile), lambda f: (0, f)),
        compiler_params=params,
        cost_estimate=pl.CostEstimate(
            flops=4 * slots * width * inner, bytes_accessed=4 * width * inner, transcendentals=0
        ),
    )
    other_gated = core_swap(twin_gated)
    y_order = (y + jnp.array([0, 1, 3, 2], jnp.int32)) % 4
    kept, up, down, far = run(
        output_kernel,
        tuple(shape((rows, width)) for _ in range(4)),
        (y_order, own_gated, other_gated, output_weight, twin_out),
        scalars=1,
        flops=2 * 4 * rows * 2 * VALUE_DIM * width,
        scratch=(pltpu.VMEM((4 * rows, VALUE_DIM), BF), pltpu.VMEM((4 * rows, VALUE_DIM), BF)),
    )
    got_up = y_shift(up, 1)
    got_down = y_shift(down, -1)
    got_far = y_shift(far, 2)
    hidden = expand(after(tokens, kept), expert_gate[0], expert_up[0], to_source)
    mixer_output = run(sum_kernel, shape((rows, width)), (kept, got_up, got_down, got_far))

    project_down = pl.pallas_call(
        down_kernel,
        grid=(width // wide,),
        out_shape=shape((n_ep * n_tp, CAP, width)),
        in_specs=[
            pl.BlockSpec((slots, inner), lambda f: (0, 0)),
            pl.BlockSpec((inner, wide), lambda f: (0, f)),
        ],
        out_specs=pl.BlockSpec((n_ep * n_tp, CAP, wide), lambda f: (0, 0, f)),
        compiler_params=params,
        cost_estimate=pl.CostEstimate(
            flops=2 * slots * width * inner, bytes_accessed=2 * width * inner, transcendentals=0
        ),
    )
    results = project_down(hidden, expert_down[0])
    returned = exchange(results, ("ep", "tp"))
    columns = jnp.stack([index // CAP, index % CAP])
    expert_output = run(
        combine_kernel,
        shape((rows, width)),
        (returned, routes, group_weight[:, None], pair_weight, columns),
        flops=4 * slots * rows * width,
    )
    return (mixer_output, expert_output)


def solution(mesh):
    both = ("ep", "tp")
    return jax.shard_map(
        local,
        mesh=mesh,
        in_specs=(
            P(both, None),
            P("ep", "tp"),
            P(),
            P(None, "tp"),
            P(None, "tp"),
            P(None, "tp"),
            P(None, "tp"),
            P("tp"),
            P("tp", None),
            P(both, None),
            P(),
            P(both, None),
            P(both),
            P(both, None),
            P(both, None, None),
            P(both, None, None),
            P(both, None, None),
        ),
        out_specs=(P(both, None), P(both, None)),
        check_vma=False,
    )
```

profile of v0, /device:TPU:1, one launch (start us, length us, event | category | flops | bytes accessed | tf_op | source)
XLA Modules:
  0.0 162.1 jit_solution(18069158058288795485)
XLA Ops:
  0.6 2.2 %shard_map.212.refs_0_ = bf16[128,2048]{1,0:T(8,128)(2,1)} custom-call(bf16[128,2048]{1,0:T(8,128)(2,1)} %x_hbm.1, f32[1,2048]{1,0:T(1,128)} %bitcast.16), custom_call_target="tpu_custom_call" | custom-call | bytes 1056768 | tf_op jit(solution)/shard_map/pallas_call | solution.py:28
  2.8 3.1 %shard_map.219 = bf16[16,3,8,2048]{3,2,1,0:T(8,128)(2,1)} custom-call(bf16[128,2048]{1,0:T(8,128)(2,1)} %x_hbm.2, f32[1,2048]{1,0:T(1,128)} %bitcast.17, s32[2,128]{1,0:T(2,128)} %bitcast.18), custom_call_target="tpu_custom_call" | custom-call | flops 201326592 | bytes 2106368 | tf_op jit(solution)/shard_map/pallas_call | solution.py:28
  6.0 8.6 %all-to-all-start = ((bf16[16,3,8,2048]{3,2,1,0:T(8,128)(2,1)}), bf16[16,3,8,2048]{3,2,1,0:T(8,128)(2,1)S(1)}, u32[]{:S(2)}, u32[]{:S(2)}) async-start(bf16[16,3,8,2048]{3,2,1,0:T(8,128)(2,1)} %shard_map.219), calls=%async_computation | async-start | bytes 3145728 | tf_op jit(solution)/shard_map/all_to_all | solution.py:307
  16.0 1.5 collective-permute-start.3
  18.9 1.7 %collective-permute-start.5 = (bf16[128,2048]{1,0:T(8,128)(2,1)S(1)}, bf16[128,2048]{1,0:T(8,128)(2,1)S(1)}, u32[]{:S(2)}, u32[]{:S(2)}) collective-permute-start(bf16[128,2048]{1,0:T(8,128)(2,1)S(1)} %copy-done.2), channel_id=1, source_target_pairs={{0,4},{1,5},{2,6},{3,7},{4,0},{5,1},{6,2},{7,3},{8,12},{9,13},{10,... | collective-permute-start | bytes 1572872 | tf_op jit(solution)/shard_map/ppermute | solution.py:295
  21.8 1.9 %multiply_cosine_fusion = (f32[1024,64]{1,0:T(8,128)S(1)}, f32[1024,64]{1,0:T(8,128)S(1)}) fusion(f32[64]{0:T(128)S(1)} %multiply_power_fusion, f32[1024]{0:T(1024)S(1)} %add_convert_fusion), kind=kLoop, calls=%fused_computation.1 | loop fusion | flops 65536 | bytes 528640 | tf_op jit(solution)/shard_map/cos | solution.py:315
  23.9 4.7 %collective-permute-done.1.refs_2_ = bf16[128,2048]{1,0:T(8,128)(2,1)} collective-permute-done((bf16[128,2048]{1,0:T(8,128)(2,1)S(1)}, bf16[128,2048]{1,0:T(8,128)(2,1)}, u32[]{:S(2)}, u32[]{:S(2)}) %collective-permute-start.1) | collective-permute-done | bytes 524320 | tf_op jit(solution)/shard_map/ppermute | solution.py:295
  28.6 2.0 %collective-permute-start.2 = (bf16[128,2048]{1,0:T(8,128)(2,1)}, bf16[128,2048]{1,0:T(8,128)(2,1)S(1)}, u32[]{:S(2)}, u32[]{:S(2)}) collective-permute-start(bf16[128,2048]{1,0:T(8,128)(2,1)} %collective-permute-done.1.refs_2_), channel_id=1, source_target_pairs={{0,1},{1,0},{2,3},{3,2},{4,5},{5,4},{6,7},{7,6},{8,9},{9,8},{10,11... | collective-permute-start | bytes 1572872 | tf_op jit(solution)/shard_map/ppermute | solution.py:291
  30.6 10.3 %collective-permute-start.4 = (bf16[128,2048]{1,0:T(8,128)(2,1)}, bf16[128,2048]{1,0:T(8,128)(2,1)S(1)}, u32[]{:S(2)}, u32[]{:S(2)}) collective-permute-start(bf16[128,2048]{1,0:T(8,128)(2,1)} %collective-permute-done.3.refs_4_), channel_id=1, source_target_pairs={{0,1},{1,0},{2,3},{3,2},{4,5},{5,4},{6,7},{7,6},{8,9},{9,8},{10,11... | collective-permute-start | bytes 1572872 | tf_op jit(solution)/shard_map/ppermute | solution.py:291
  40.9 1.8 %collective-permute-start.6 = (bf16[128,2048]{1,0:T(8,128)(2,1)S(1)}, bf16[128,2048]{1,0:T(8,128)(2,1)S(1)}, u32[]{:S(2)}, u32[]{:S(2)}) collective-permute-start(bf16[128,2048]{1,0:T(8,128)(2,1)S(1)} %collective-permute-done.5.b0_ref), channel_id=1, source_target_pairs={{0,1},{1,0},{2,3},{3,2},{4,5},{5,4},{6,7},{7,6},{8,9},{9,8},{10,11... | collective-permute-start | bytes 1572872 | tf_op jit(solution)/shard_map/ppermute | solution.py:291
  44.0 4.5 %shard_map.213 = (bf16[768,768]{1,0:T(8,128)(2,1)S(1)}, bf16[2048,768]{1,0:T(8,128)(2,1)S(1)}) custom-call(bf16[128,2048]{1,0:T(8,128)(2,1)S(1)} %copy-done.2, bf16[128,2048]{1,0:T(8,128)(2,1)} %collective-permute-done.refs_1_, bf16[128,2048]{1,0:T(8,128)(2,1)} %collective-permute-done.1.refs_2_, bf16[128,2048]{1,0:T(8,128)(2,1)S(1)} %collective-permute-done.2.refs_3_, ...), custom_call_target="tpu_custom_call" | custom-call | flops 2415919104 | bytes 10616832 | tf_op jit(solution)/shard_map/pallas_call | solution.py:28
  49.5 3.4 %shard_map.214 = (bf16[1024,256]{1,0:T(8,128)(2,1)S(1)}, bf16[136,256]{1,0:T(8,128)(2,1)S(1)}, f32[1024,256]{1,0:T(8,128)S(1)}, bf16[1024,128]{1,0:T(8,128)(2,1)S(1)}) custom-call(s32[8]{0:T(128)S(1)} %fusion.22.src_ref, bf16[768,768]{1,0:T(8,128)(2,1)S(1)} %get-tuple-element.20.early_ref, bf16[128,2048]{1,0:T(8,128)(2,1)S(1)} %copy-done.1, ...), custom_call_target="tpu_custom_call" | custom-call | flops 805306368 | bytes 7811104 | tf_op jit(solution)/shard_map/pallas_call | solution.py:28
  53.7 2.1 %shard_map.220 = bf16[384,2048]{1,0:T(8,128)(2,1)} custom-call(bf16[384,384]{1,0:T(8,128)(2,1)S(1)} %fusion.perm_ref, bf16[384,2048]{1,0:T(8,128)(2,1)S(1)} %bitcast.13), custom_call_target="tpu_custom_call" | custom-call | flops 603979776 | bytes 3440640 | tf_op jit(solution)/shard_map/pallas_call | solution.py:28
  55.8 5.3 %all-to-all-start.1 = ((bf16[8,48,2048]{2,1,0:T(8,128)(2,1)}), bf16[8,48,2048]{2,1,0:T(8,128)(2,1)}, u32[]{:S(2)}, u32[]{:S(2)}) async-start(bf16[8,48,2048]{2,1,0:T(8,128)(2,1)} %bitcast.6), calls=%async_computation.1 | async-start | bytes 3145728 | tf_op jit(solution)/shard_map/all_to_all | solution.py:307
  61.2 1.5 collective-permute-start.7
  64.1 1.7 %collective-permute-start.9 = (bf16[136,256]{1,0:T(8,128)(2,1)S(1)}, bf16[136,256]{1,0:T(8,128)(2,1)S(1)}, u32[]{:S(2)}, u32[]{:S(2)}) collective-permute-start(bf16[136,256]{1,0:T(8,128)(2,1)S(1)} %get-tuple-element.22.p0), channel_id=1, source_target_pairs={{0,16},{8,24},{16,0},{24,8},{32,48},{40,56},{48,32},{56,40},{64,80... | collective-permute-start | bytes 208904 | tf_op jit(solution)/shard_map/ppermute | solution.py:299
  66.3 2.8 %collective-permute-done.9.p3 = bf16[136,256]{1,0:T(8,128)(2,1)S(1)} collective-permute-done((bf16[136,256]{1,0:T(8,128)(2,1)S(1)}, bf16[136,256]{1,0:T(8,128)(2,1)S(1)}, u32[]{:S(2)}, u32[]{:S(2)}) %collective-permute-start.9) | collective-permute-done | bytes 69664 | tf_op jit(solution)/shard_map/ppermute | solution.py:299
  69.8 1.4 collective-permute-start.10
  72.6 1.7 %collective-permute-start.12 = (bf16[136,256]{1,0:T(8,128)(2,1)S(1)}, bf16[136,256]{1,0:T(8,128)(2,1)S(1)}, u32[]{:S(2)}, u32[]{:S(2)}) collective-permute-start(bf16[136,256]{1,0:T(8,128)(2,1)S(1)} %get-tuple-element.23.p0), channel_id=1, source_target_pairs={{0,64},{8,72},{16,80},{24,88},{32,96},{40,104},{48,112},{56,120},{... | collective-permute-start | bytes 208904 | tf_op jit(solution)/shard_map/ppermute | solution.py:303
  74.8 3.1 %collective-permute-done.12.p3 = bf16[136,256]{1,0:T(8,128)(2,1)S(1)} collective-permute-done((bf16[136,256]{1,0:T(8,128)(2,1)S(1)}, bf16[136,256]{1,0:T(8,128)(2,1)S(1)}, u32[]{:S(2)}, u32[]{:S(2)}) %collective-permute-start.12) | collective-permute-done | bytes 69664 | tf_op jit(solution)/shard_map/ppermute | solution.py:303
  77.9 1.4 shard_map.216
  79.3 2.7 %collective-permute-start.13 = (bf16[512,256]{1,0:T(8,128)(2,1)S(1)}, bf16[512,256]{1,0:T(8,128)(2,1)S(1)}, u32[]{:S(2)}, u32[]{:S(2)}) collective-permute-start(bf16[512,256]{1,0:T(8,128)(2,1)S(1)} %get-tuple-element.30), channel_id=1, source_target_pairs={{0,1},{1,0},{2,3},{3,2},{4,5},{5,4},{6,7},{7,6},{8,9},{9,8},{10,11... | collective-permute-start | bytes 786440 | tf_op jit(solution)/shard_map/ppermute | solution.py:291
  83.2 2.5 %shard_map.217 = (bf16[128,2048]{1,0:T(8,128)(2,1)S(1)}, bf16[128,2048]{1,0:T(8,128)(2,1)S(1)}, bf16[128,2048]{1,0:T(8,128)(2,1)S(1)}, bf16[128,2048]{1,0:T(8,128)(2,1)S(1)}) custom-call(s32[4]{0:T(128)S(1)} %and_select_fusion.6.y_ref, bf16[512,256]{1,0:T(8,128)(2,1)S(1)} %get-tuple-element.29.own_ref, ...), custom_call_target="tpu_custom_call" | custom-call | flops 1073741824 | bytes 4718608 | tf_op jit(solution)/shard_map/pallas_call | solution.py:28
  87.3 8.9 %shard_map.221.h_ref = bf16[384,1024]{1,0:T(8,128)(2,1)} custom-call(bf16[384,2048]{1,0:T(8,128)(2,1)} %bitcast.7.x_ref, bf16[2048,1024]{1,0:T(8,128)(2,1)} %bitcast.20, bf16[2048,1024]{1,0:T(8,128)(2,1)} %bitcast.21, bf16[384,384]{1,0:T(8,128)(2,1)} %fusion.1.perm_ref), custom_call_target="tpu_custom_call" | custom-call | flops 3221225472 | bytes 8388608 | tf_op jit(solution)/shard_map/pallas_call | solution.py:478
  96.2 6.4 %shard_map.222 = bf16[128,3,2048]{2,1,0:T(4,128)(2,1)} custom-call(bf16[384,1024]{1,0:T(8,128)(2,1)} %shard_map.221.h_ref, bf16[1024,2048]{1,0:T(8,128)(2,1)} %bitcast.15), custom_call_target="tpu_custom_call" | custom-call | flops 1610612736 | bytes 4194304 | tf_op jit(solution)/shard_map/pallas_call | solution.py:495
  102.6 7.1 %all-to-all-start.2 = ((bf16[128,3,2048]{2,1,0:T(4,128)(2,1)}), bf16[128,3,2048]{2,1,0:T(4,128)(2,1)S(1)}, u32[]{:S(2)}, u32[]{:S(2)}) async-start(bf16[128,3,2048]{2,1,0:T(4,128)(2,1)} %shard_map.222), calls=%async_computation.2 | async-start | bytes 4194304 | tf_op jit(solution)/shard_map/all_to_all | solution.py:307
  109.7 1.4 collective-permute-start.15
  112.5 1.6 %collective-permute-start.17 = (bf16[128,2048]{1,0:T(8,128)(2,1)}, bf16[128,2048]{1,0:T(8,128)(2,1)}, u32[]{:S(2)}, u32[]{:S(2)}) collective-permute-start(bf16[128,2048]{1,0:T(8,128)(2,1)} %copy-done.11), channel_id=1, source_target_pairs={{0,4},{1,5},{2,6},{3,7},{4,0},{5,1},{6,2},{7,3},{8,12},{9,13},{10,... | collective-permute-start | bytes 1572872 | tf_op jit(solution)/shard_map/ppermute | solution.py:295
  114.5 31.5 %collective-permute-done.15.b = bf16[128,2048]{1,0:T(8,128)(2,1)S(1)} collective-permute-done((bf16[128,2048]{1,0:T(8,128)(2,1)}, bf16[128,2048]{1,0:T(8,128)(2,1)S(1)}, u32[]{:S(2)}, u32[]{:S(2)}) %collective-permute-start.15) | collective-permute-done | bytes 524320 | tf_op jit(solution)/shard_map/ppermute | solution.py:295
  146.0 11.9 %collective-permute-done.17.d = bf16[128,2048]{1,0:T(8,128)(2,1)} collective-permute-done((bf16[128,2048]{1,0:T(8,128)(2,1)}, bf16[128,2048]{1,0:T(8,128)(2,1)}, u32[]{:S(2)}, u32[]{:S(2)}) %collective-permute-start.17) | collective-permute-done | bytes 524320 | tf_op jit(solution)/shard_map/ppermute | solution.py:295
  157.9 2.2 %shard_map.218 = bf16[128,2048]{1,0:T(8,128)(2,1)} custom-call(bf16[128,2048]{1,0:T(8,128)(2,1)S(1)} %get-tuple-element.31.a, bf16[128,2048]{1,0:T(8,128)(2,1)S(1)} %collective-permute-done.15.b, bf16[128,2048]{1,0:T(8,128)(2,1)} %collective-permute-done.16.c, bf16[128,2048]{1,0:T(8,128)(2,1)} %collective-permute-done.17.d), custom_call_target="tpu_custom_call" | custom-call | bytes 2621440 | tf_op jit(solution)/shard_map/pallas_call | solution.py:28
  160.1 2.0 %shard_map.223 = bf16[128,2048]{1,0:T(8,128)(2,1)} custom-call(bf16[128,3,2048]{2,1,0:T(4,128)(2,1)S(1)} %all-to-all-done.2.rows_ref, s32[128,2]{1,0:T(8,128)S(1)} %copy.23.routes_ref, f32[128,1]{1,0:T(8,128)S(1)} %copy.24.group_ref, f32[128,2]{1,0:T(8,128)S(1)} %copy.25.pair_ref, s32[2,384]{1,0:T(2,128)S(1)} %pad_add_fusion.cols_ref), custom_call_target="tpu_custom_call" | custom-call | flops 402653184 | bytes 2102784 | tf_op jit(solution)/shard_map/pallas_call | solution.py:28
  (86 shorter events, 16.2 us)
Async XLA Ops:
  6.0 15.1 %copy-start.15 = (f32[1024,1]{0,1:T(1,128)S(1)}, f32[1024,1]{0,1:T(1,128)}, u32[]{:S(2)}) copy-start(f32[1024,1]{0,1:T(1,128)} %param.22) | copy-start | bytes 12292
  6.0 47.7 %all-to-all-start = ((bf16[16,3,8,2048]{3,2,1,0:T(8,128)(2,1)}), bf16[16,3,8,2048]{3,2,1,0:T(8,128)(2,1)S(1)}, u32[]{:S(2)}, u32[]{:S(2)}) async-start(bf16[16,3,8,2048]{3,2,1,0:T(8,128)(2,1)} %shard_map.219), calls=%async_computation | async-start | bytes 3145728 | tf_op jit(solution)/shard_map/all_to_all | solution.py:307
  14.6 26.3 %copy-start.19 = (s32[8]{0:T(128)S(1)}, s32[8]{0:T(128)}, u32[]{:S(2)}) copy-start(s32[8]{0:T(128)} %constant.155.clone) | copy-start | bytes 100
  14.6 26.3 %copy-start.20 = (s32[8]{0:T(128)S(1)}, s32[8]{0:T(128)}, u32[]{:S(2)}) copy-start(s32[8]{0:T(128)} %constant.156.clone) | copy-start | bytes 100
  14.6 28.3 %copy-start.9 = (bf16[2048,128]{1,0:T(8,128)(2,1)S(1)}, bf16[2048,128]{1,0:T(8,128)(2,1)}, u32[]{:S(2)}) copy-start(bf16[2048,128]{1,0:T(8,128)(2,1)} %refs_6_.1) | copy-start | bytes 1572868
  14.6 14.0 %collective-permute-start.1 = (bf16[128,2048]{1,0:T(8,128)(2,1)S(1)}, bf16[128,2048]{1,0:T(8,128)(2,1)}, u32[]{:S(2)}, u32[]{:S(2)}) collective-permute-start(bf16[128,2048]{1,0:T(8,128)(2,1)S(1)} %copy-done.2), channel_id=1, source_target_pairs={{0,2},{1,3},{2,4},{3,5},{4,6},{5,7},{6,0},{7,1},{8,10},{9,11},{10,... | collective-permute-start | bytes 1572872 | tf_op jit(solution)/shard_map/ppermute | solution.py:295
  16.0 14.7 %collective-permute-start.3 = (bf16[128,2048]{1,0:T(8,128)(2,1)S(1)}, bf16[128,2048]{1,0:T(8,128)(2,1)}, u32[]{:S(2)}, u32[]{:S(2)}) collective-permute-start(bf16[128,2048]{1,0:T(8,128)(2,1)S(1)} %copy-done.2), channel_id=1, source_target_pairs={{0,6},{1,7},{2,0},{3,1},{4,2},{5,3},{6,4},{7,5},{8,14},{9,15},{10,... | collective-permute-start | bytes 1572872 | tf_op jit(solution)/shard_map/ppermute | solution.py:295
  17.5 25.4 %collective-permute-start = (bf16[128,2048]{1,0:T(8,128)(2,1)S(1)}, bf16[128,2048]{1,0:T(8,128)(2,1)}, u32[]{:S(2)}, u32[]{:S(2)}) collective-permute-start(bf16[128,2048]{1,0:T(8,128)(2,1)S(1)} %copy-done.2), channel_id=1, source_target_pairs={{0,1},{1,0},{2,3},{3,2},{4,5},{5,4},{6,7},{7,6},{8,9},{9,8},{10,11... | collective-permute-start | bytes 1572872 | tf_op jit(solution)/shard_map/ppermute | solution.py:291
  18.9 22.0 %collective-permute-start.5 = (bf16[128,2048]{1,0:T(8,128)(2,1)S(1)}, bf16[128,2048]{1,0:T(8,128)(2,1)S(1)}, u32[]{:S(2)}, u32[]{:S(2)}) collective-permute-start(bf16[128,2048]{1,0:T(8,128)(2,1)S(1)} %copy-done.2), channel_id=1, source_target_pairs={{0,4},{1,5},{2,6},{3,7},{4,0},{5,1},{6,2},{7,3},{8,12},{9,13},{10,... | collective-permute-start | bytes 1572872 | tf_op jit(solution)/shard_map/ppermute | solution.py:295
  21.8 21.1 %copy-start.6 = (bf16[2048,256]{1,0:T(8,128)(2,1)S(1)}, bf16[2048,256]{1,0:T(8,128)(2,1)}, u32[]{:S(2)}) copy-start(bf16[2048,256]{1,0:T(8,128)(2,1)} %refs_8_.1) | copy-start | bytes 3145732
  21.8 21.1 %copy-start.7 = (bf16[2048,256]{1,0:T(8,128)(2,1)S(1)}, bf16[2048,256]{1,0:T(8,128)(2,1)}, u32[]{:S(2)}) copy-start(bf16[2048,256]{1,0:T(8,128)(2,1)} %refs_9_.1) | copy-start | bytes 3145732
  28.6 14.2 %collective-permute-start.2 = (bf16[128,2048]{1,0:T(8,128)(2,1)}, bf16[128,2048]{1,0:T(8,128)(2,1)S(1)}, u32[]{:S(2)}, u32[]{:S(2)}) collective-permute-start(bf16[128,2048]{1,0:T(8,128)(2,1)} %collective-permute-done.1.refs_2_), channel_id=1, source_target_pairs={{0,1},{1,0},{2,3},{3,2},{4,5},{5,4},{6,7},{7,6},{8,9},{9,8},{10,11... | collective-permute-start | bytes 1572872 | tf_op jit(solution)/shard_map/ppermute | solution.py:291
  30.6 12.2 %collective-permute-start.4 = (bf16[128,2048]{1,0:T(8,128)(2,1)}, bf16[128,2048]{1,0:T(8,128)(2,1)S(1)}, u32[]{:S(2)}, u32[]{:S(2)}) collective-permute-start(bf16[128,2048]{1,0:T(8,128)(2,1)} %collective-permute-done.3.refs_4_), channel_id=1, source_target_pairs={{0,1},{1,0},{2,3},{3,2},{4,5},{5,4},{6,7},{7,6},{8,9},{9,8},{10,11... | collective-permute-start | bytes 1572872 | tf_op jit(solution)/shard_map/ppermute | solution.py:291
  40.9 7.5 %collective-permute-start.6 = (bf16[128,2048]{1,0:T(8,128)(2,1)S(1)}, bf16[128,2048]{1,0:T(8,128)(2,1)S(1)}, u32[]{:S(2)}, u32[]{:S(2)}) collective-permute-start(bf16[128,2048]{1,0:T(8,128)(2,1)S(1)} %collective-permute-done.5.b0_ref), channel_id=1, source_target_pairs={{0,1},{1,0},{2,3},{3,2},{4,5},{5,4},{6,7},{7,6},{8,9},{9,8},{10,11... | collective-permute-start | bytes 1572872 | tf_op jit(solution)/shard_map/ppermute | solution.py:291
  55.8 18.4 %copy-start.21 = (s32[4]{0:T(128)S(1)}, s32[4]{0:T(128)}, u32[]{:S(2)}) copy-start(s32[4]{0:T(128)} %constant.158.clone) | copy-start | bytes 52
  55.8 22.1 %copy-start.4 = (bf16[1024,128]{1,0:T(8,128)(2,1)S(1)}, bf16[1024,128]{1,0:T(8,128)(2,1)}, u32[]{:S(2)}) copy-start(bf16[1024,128]{1,0:T(8,128)(2,1)} %copy-done.3) | copy-start | bytes 786436
  55.8 22.1 %copy-start.5 = (f32[256]{0:T(256)S(1)}, f32[256]{0:T(256)}, u32[]{:S(2)}) copy-start(f32[256]{0:T(256)} %param.28) | copy-start | bytes 3076
  55.8 31.5 %all-to-all-start.1 = ((bf16[8,48,2048]{2,1,0:T(8,128)(2,1)}), bf16[8,48,2048]{2,1,0:T(8,128)(2,1)}, u32[]{:S(2)}, u32[]{:S(2)}) async-start(bf16[8,48,2048]{2,1,0:T(8,128)(2,1)} %bitcast.6), calls=%async_computation.1 | async-start | bytes 3145728 | tf_op jit(solution)/shard_map/all_to_all | solution.py:307
  61.1 21.8 %collective-permute-start.14 = (bf16[256,2048]{1,0:T(8,128)(2,1)S(1)}, bf16[256,2048]{1,0:T(8,128)(2,1)}, u32[]{:S(2)}, u32[]{:S(2)}) collective-permute-start(bf16[256,2048]{1,0:T(8,128)(2,1)S(1)} %copy-done.8), channel_id=1, source_target_pairs={{0,1},{1,0},{2,3},{3,2},{4,5},{5,4},{6,7},{7,6},{8,9},{9,8},{10,11... | collective-permute-start | bytes 3145736 | tf_op jit(solution)/shard_map/ppermute | solution.py:291
  61.2 5.0 %collective-permute-start.7 = (bf16[136,256]{1,0:T(8,128)(2,1)S(1)}, bf16[136,256]{1,0:T(8,128)(2,1)S(1)}, u32[]{:S(2)}, u32[]{:S(2)}) collective-permute-start(bf16[136,256]{1,0:T(8,128)(2,1)S(1)} %get-tuple-element.22.p0), channel_id=1, source_target_pairs={{0,8},{8,16},{16,24},{24,0},{32,40},{40,48},{48,56},{56,32},{64,72... | collective-permute-start | bytes 208904 | tf_op jit(solution)/shard_map/ppermute | solution.py:299
  62.8 3.6 %collective-permute-start.8 = (bf16[136,256]{1,0:T(8,128)(2,1)S(1)}, bf16[136,256]{1,0:T(8,128)(2,1)S(1)}, u32[]{:S(2)}, u32[]{:S(2)}) collective-permute-start(bf16[136,256]{1,0:T(8,128)(2,1)S(1)} %get-tuple-element.22.p0), channel_id=1, source_target_pairs={{0,24},{8,0},{16,8},{24,16},{32,56},{40,32},{48,40},{56,48},{64,88... | collective-permute-start | bytes 208904 | tf_op jit(solution)/shard_map/ppermute | solution.py:299
  64.1 5.1 %collective-permute-start.9 = (bf16[136,256]{1,0:T(8,128)(2,1)S(1)}, bf16[136,256]{1,0:T(8,128)(2,1)S(1)}, u32[]{:S(2)}, u32[]{:S(2)}) collective-permute-start(bf16[136,256]{1,0:T(8,128)(2,1)S(1)} %get-tuple-element.22.p0), channel_id=1, source_target_pairs={{0,16},{8,24},{16,0},{24,8},{32,48},{40,56},{48,32},{56,40},{64,80... | collective-permute-start | bytes 208904 | tf_op jit(solution)/shard_map/ppermute | solution.py:299
  69.8 4.8 %collective-permute-start.10 = (bf16[136,256]{1,0:T(8,128)(2,1)S(1)}, bf16[136,256]{1,0:T(8,128)(2,1)S(1)}, u32[]{:S(2)}, u32[]{:S(2)}) collective-permute-start(bf16[136,256]{1,0:T(8,128)(2,1)S(1)} %get-tuple-element.23.p0), channel_id=1, source_target_pairs={{0,32},{8,40},{16,48},{24,56},{32,64},{40,72},{48,80},{56,88},{64,... | collective-permute-start | bytes 208904 | tf_op jit(solution)/shard_map/ppermute | solution.py:303
  71.3 3.6 %collective-permute-start.11 = (bf16[136,256]{1,0:T(8,128)(2,1)S(1)}, bf16[136,256]{1,0:T(8,128)(2,1)S(1)}, u32[]{:S(2)}, u32[]{:S(2)}) collective-permute-start(bf16[136,256]{1,0:T(8,128)(2,1)S(1)} %get-tuple-element.23.p0), channel_id=1, source_target_pairs={{0,96},{8,104},{16,112},{24,120},{32,0},{40,8},{48,16},{56,24},{64... | collective-permute-start | bytes 208904 | tf_op jit(solution)/shard_map/ppermute | solution.py:303
  72.6 5.3 %collective-permute-start.12 = (bf16[136,256]{1,0:T(8,128)(2,1)S(1)}, bf16[136,256]{1,0:T(8,128)(2,1)S(1)}, u32[]{:S(2)}, u32[]{:S(2)}) collective-permute-start(bf16[136,256]{1,0:T(8,128)(2,1)S(1)} %get-tuple-element.23.p0), channel_id=1, source_target_pairs={{0,64},{8,72},{16,80},{24,88},{32,96},{40,104},{48,112},{56,120},{... | collective-permute-start | bytes 208904 | tf_op jit(solution)/shard_map/ppermute | solution.py:303
  79.3 3.9 %collective-permute-start.13 = (bf16[512,256]{1,0:T(8,128)(2,1)S(1)}, bf16[512,256]{1,0:T(8,128)(2,1)S(1)}, u32[]{:S(2)}, u32[]{:S(2)}) collective-permute-start(bf16[512,256]{1,0:T(8,128)(2,1)S(1)} %get-tuple-element.30), channel_id=1, source_target_pairs={{0,1},{1,0},{2,3},{3,2},{4,5},{5,4},{6,7},{7,6},{8,9},{9,8},{10,11... | collective-permute-start | bytes 786440 | tf_op jit(solution)/shard_map/ppermute | solution.py:291
  87.3 15.3 %copy-start.12 = (bf16[128,2048]{1,0:T(8,128)(2,1)}, bf16[128,2048]{1,0:T(8,128)(2,1)S(1)}, u32[]{:S(2)}) copy-start(bf16[128,2048]{1,0:T(8,128)(2,1)S(1)} %get-tuple-element.33) | copy-start | bytes 1572868
  102.6 11.8 %copy-start.16 = (f32[128,2]{0,1:T(2,128)S(1)}, f32[128,2]{0,1:T(2,128)}, u32[]{:S(2)}) copy-start(f32[128,2]{0,1:T(2,128)} %param.34) | copy-start | bytes 3076
  102.6 57.6 %all-to-all-start.2 = ((bf16[128,3,2048]{2,1,0:T(4,128)(2,1)}), bf16[128,3,2048]{2,1,0:T(4,128)(2,1)S(1)}, u32[]{:S(2)}, u32[]{:S(2)}) async-start(bf16[128,3,2048]{2,1,0:T(4,128)(2,1)} %shard_map.222), calls=%async_computation.2 | async-start | bytes 4194304 | tf_op jit(solution)/shard_map/all_to_all | solution.py:307
  109.7 36.3 %collective-permute-start.15 = (bf16[128,2048]{1,0:T(8,128)(2,1)}, bf16[128,2048]{1,0:T(8,128)(2,1)S(1)}, u32[]{:S(2)}, u32[]{:S(2)}) collective-permute-start(bf16[128,2048]{1,0:T(8,128)(2,1)} %copy-done.13), channel_id=1, source_target_pairs={{0,2},{1,3},{2,4},{3,5},{4,6},{5,7},{6,0},{7,1},{8,10},{9,11},{10,... | collective-permute-start | bytes 1572872 | tf_op jit(solution)/shard_map/ppermute | solution.py:295
  111.1 34.9 %collective-permute-start.16 = (bf16[128,2048]{1,0:T(8,128)(2,1)}, bf16[128,2048]{1,0:T(8,128)(2,1)}, u32[]{:S(2)}, u32[]{:S(2)}) collective-permute-start(bf16[128,2048]{1,0:T(8,128)(2,1)} %copy-done.12), channel_id=1, source_target_pairs={{0,6},{1,7},{2,0},{3,1},{4,2},{5,3},{6,4},{7,5},{8,14},{9,15},{10,... | collective-permute-start | bytes 1572872 | tf_op jit(solution)/shard_map/ppermute | solution.py:295
  112.5 45.4 %collective-permute-start.17 = (bf16[128,2048]{1,0:T(8,128)(2,1)}, bf16[128,2048]{1,0:T(8,128)(2,1)}, u32[]{:S(2)}, u32[]{:S(2)}) collective-permute-start(bf16[128,2048]{1,0:T(8,128)(2,1)} %copy-done.11), channel_id=1, source_target_pairs={{0,4},{1,5},{2,6},{3,7},{4,0},{5,1},{6,2},{7,3},{8,12},{9,13},{10,... | collective-permute-start | bytes 1572872 | tf_op jit(solution)/shard_map/ppermute | solution.py:295
  (11 other events, 59.0 us)
where the time goes:
time: 163 us; the launch traced here: 162 us
  starting transfers between devices  57.1 us (35%)
  waiting for transfers between devices  55.4 us (34%)
  Pallas kernels  39.5 us (24%)
  local copies, waits for them, and re-layouts  5.31 us (3%)
  other arithmetic  3.82 us (2%)
    ppermute x6, waiting for transfers between devices, y_shift(): lax.ppermute(x, 'tp', [(t, (t // 2 + k) % 4 * 2 + t % 2) for t in range(8)])  48.1 us
    pallas_call x10, Pallas kernels, run(): pl.pallas_call(kernel, out_shape=outs, in_specs=[SM if i < scalars else H...  24.2 us
    all_to_all x3, starting transfers between devices, exchange(): return lax.all_to_all(x, axis, split_axis=0, concat_axis=0, tiled=True)  21 us
    ppermute x6, starting transfers between devices, core_swap(): return lax.ppermute(x, 'tp', [(t, t ^ 1) for t in range(8)])  18.2 us
    ppermute x6, starting transfers between devices, y_shift(): lax.ppermute(x, 'tp', [(t, (t // 2 + k) % 4 * 2 + t % 2) for t in range(8)])  8.97 us
    pallas_call x1, Pallas kernels, local(): expand(after(tokens, kept), expert_gate[0], expert_up[0], to_source)  8.89 us
    pallas_call x1, Pallas kernels, local(): results = project_down(hidden, expert_down[0])  6.38 us
    unnamed x47, local copies, waits for them, and re-layouts  5.18 us
  transfers between devices with their start and end apart: 21, of which 10 were waited for; matrix products, arithmetic and copies ran while one was open for 3% of the time, Pallas kernels for 9%

commit v1 on v0

--- a/solution.py
+++ b/solution.py
@@ -1,5 +1,8 @@
+import functools
+
 import jax
 import jax.numpy as jnp
+import numpy as np
 from jax import lax
 from jax.experimental import pallas as pl
 from jax.experimental.pallas import tpu as pltpu
@@ -21,7 +24,7 @@
 HBM = pl.BlockSpec(memory_space=pltpu.HBM)
 
 
-def run(kernel, outs, args, scalars=0, flops=0, scratch=(), vmem=24 << 20, hbm=()):
+def run(kernel, outs, args, scalars=0, flops=0, scratch=(), vmem=24 << 20, hbm=(), hbm_outs=()):
     nbytes = sum(a.size * a.dtype.itemsize for a in args) + sum(
         o.size * o.dtype.itemsize for o in jax.tree.leaves(outs)
     )
@@ -29,7 +32,9 @@
         kernel,
         out_shape=outs,
         in_specs=[SM if i < scalars else HBM if i in hbm else VM for i in range(len(args))],
-        out_specs=jax.tree.map(lambda _: VM, outs),
+        out_specs=tuple(HBM if i in hbm_outs else VM for i in range(len(outs)))
+        if isinstance(outs, tuple)
+        else VM,
         scratch_shapes=list(scratch),
         compiler_params=pltpu.CompilerParams(vmem_limit_bytes=vmem),
         cost_estimate=pl.CostEstimate(flops=flops, bytes_accessed=nbytes, transcendentals=0),
@@ -59,12 +64,28 @@
     return centred * lax.rsqrt(spread + EPSILON) * gain
 
 
-def fetch(sems, *pairs):
+def begin(sems, *pairs):
     copies = [pltpu.make_async_copy(a, b, sems.at[i]) for i, (a, b) in enumerate(pairs)]
     for copy in copies:
         copy.start()
+    return copies
+
+
+def finish(copies):
     for copy in copies:
         copy.wait()
+
+
+def fetch(sems, *pairs):
+    finish(begin(sems, *pairs))
+
+
+def rows_of(ref, parts):
+    pairs, lower = [], 0
+    for part in parts:
+        pairs.append((part, ref.at[lower : lower + part.shape[0], :]))
+        lower += part.shape[0]
+    return pairs
 
 
 def norm_kernel(x_hbm, gain_hbm, o_ref, x_ref, gain_ref, sems):
@@ -91,18 +112,25 @@
         )
 
 
-def permute_kernel(perm_ref, x_ref, o_ref):
-    o_ref[...] = dot(perm_ref[...], x_ref[...]).astype(BF)
-
-
-def hidden_kernel(x_ref, gate_ref, up_ref, perm_ref, o_ref):
-    x = x_ref[...]
-    hidden = (silu(dot(x, gate_ref[...])) * dot(x, up_ref[...])).astype(BF)
-    o_ref[...] = dot(perm_ref[...], hidden).astype(BF)
-
-
-def down_kernel(h_ref, down_ref, o_ref):
-    o_ref[...] = dot(h_ref[...], down_ref[...]).reshape(o_ref.shape).astype(BF)
+def turn_kernel(index_ref, x_ref, o_ref):
+    rows = x_ref.shape[0]
+    perm = lax.broadcasted_iota(jnp.int32, (rows, rows), 0) == index_ref[...]
+    o_ref[...] = dot(jnp.where(perm, 1.0, 0.0).astype(BF), x_ref[...]).astype(BF)
+
+
+def expert_kernel(first, x_ref, gate_ref, up_ref, down_ref, o_ref, hidden):
+    step = pl.program_id(0)
+
+    @pl.when(step < first)
+    def _():
+        x = x_ref[...]
+        tile = gate_ref.shape[1]
+        here = pl.ds(pl.multiple_of(step * tile, tile), tile)
+        hidden[:, here] = (silu(dot(x, gate_ref[...])) * dot(x, up_ref[...])).astype(BF)
+
+    @pl.when(step >= first)
+    def _():
+        o_ref[...] = dot(hidden[...], down_ref[...]).reshape(o_ref.shape).astype(BF)
 
 
 def combine_kernel(rows_ref, routes_ref, group_ref, pair_ref, cols_ref, o_ref):
@@ -126,19 +154,18 @@
 
 
 def project_kernel(*refs):
-    *blocks, wq, wk, wv, wg, o_ref, w_ref, lhs, sems = refs
-    copies, lower = [], 0
-    for i, part in enumerate((wq, wk, wv, wg)):
-        there = w_ref.at[:, lower : lower + part.shape[1]]
-        copies.append(pltpu.make_async_copy(part, there, sems.at[i]))
+    *ins, o_hbm, w_hbm, lhs, wq, wk, wv, wg, w_ref, o_ref, sems, out_sems = refs
+    weights = begin(sems, *zip(ins[6:], (wq, wk, wv, wg)), *rows_of(lhs, ins[:6]))
+    finish(weights[:4])
+    lower = 0
+    for part in (wq, wk, wv, wg):
+        w_ref[:, lower : lower + part.shape[1]] = part[...]
         lower += part.shape[1]
-    for copy in copies:
-        copy.start()
-    for i, block in enumerate(blocks):
-        lhs[pl.ds(i * block.shape[0], block.shape[0]), :] = block[...]
-    for copy in copies:
-        copy.wait()
+    joined = begin(out_sems, (w_ref, w_hbm))
+    finish(weights[4:])
     o_ref[...] = dot(lhs[...], w_ref[...]).astype(BF)
+    fetch(sems, (o_ref, o_hbm))
+    finish(joined)
 
 
 def split_total(total, like):
@@ -158,36 +185,56 @@
     )
 
 
+AWAY = (0, 3, 1, 2)
+
+
 def mixer_kernel(
-    src_ref, early_ref, b0_ref, b1_ref, w_ref, turn_ref, decay_ref,
-    g_ref, state_ref, local_ref, scaled_ref, lhs, buf,
+    me_ref, early_hbm, b0, b1, b2, b3, w_hbm, cos_hbm, sin_hbm, cos0, sin0, decay,
+    g_hbm, state_ref, local_hbm, scaled_hbm,
+    lhs, buf, early_ref, w_ref, cos_ref, sin_ref, cos0_ref, sin0_ref, decay_ref, steps_ref,
+    local_ref, scaled_ref, g_ref, sems, late_sems,
 ):
-    rows = b0_ref.shape[0]
-    lhs[0:rows, :] = b0_ref[...]
-    lhs[rows : 2 * rows, :] = b1_ref[...]
+    first = begin(sems, (w_hbm, w_ref), *rows_of(lhs, (b0, b1, b2, b3)))
+    second = begin(
+        late_sems,
+        (early_hbm, early_ref),
+        (cos_hbm, cos_ref),
+        (sin_hbm, sin_ref),
+        (cos0, cos0_ref),
+        (sin0, sin0_ref),
+        (decay, decay_ref),
+    )
+    segment, mine = me_ref[0], me_ref[1]
+    y, core = mine // 2, mine % 2
+    rows = 2 * b0.shape[0]
+    finish(first)
     late = dot(lhs[...], w_ref[...]).astype(BF)
+    finish(second)
     early = early_ref.shape[0] // rows
     for i in range(early + 2):
-        here = pl.ds(pl.multiple_of(src_ref[i] * rows, rows), rows)
+        owner = (y + AWAY[i // 2]) % 4 * 2 + (core + i) % 2
+        here = pl.ds(pl.multiple_of(owner * rows, rows), rows)
         if i < early:
             buf[here, :] = early_ref[i * rows : (i + 1) * rows, :]
         else:
             buf[here, :] = late[(i - early) * rows : (i - early + 1) * rows, :]
     g_ref[...] = buf[:, 2 * KEY_DIM + VALUE_DIM :]
 
-    sums = prefix_sums(decay_ref[...])
+    steps_ref[...] = jnp.zeros(steps_ref.shape, F32)
+    for i in range(buf.shape[0] // CHUNK):
+        steps_ref[i : i + 1, :] = decay_ref[:, i * CHUNK : (i + 1) * CHUNK]
+    sums = prefix_sums(steps_ref[...])
+    start_cos = cos0_ref[pl.ds(segment, 1), :]
+    start_sin = sin0_ref[pl.ds(segment, 1), :]
     columns = sums.T
     causal = lax.broadcasted_iota(jnp.int32, (CHUNK, CHUNK), 0) >= lax.broadcasted_iota(
         jnp.int32, (CHUNK, CHUNK), 1
     )
-    first = lax.broadcasted_iota(jnp.int32, (CHUNK, KEY_DIM), 1) < KEY_DIM // 2
     state, base = None, jnp.zeros((1, 1), F32)
     for i in range(buf.shape[0] // CHUNK):
         here = slice(i * CHUNK, (i + 1) * CHUNK)
-        turn = turn_ref[here, :]
-        other = pltpu.roll(turn, KEY_DIM // 2, 1)
-        cosine = jnp.where(first, turn, other)
-        sine = jnp.where(first, -other, turn)
+        cosine = cos_ref[here, :] * start_cos - sin_ref[here, :] * start_sin
+        sine = sin_ref[here, :] * start_cos + cos_ref[here, :] * start_sin
 
         def rotated(lower):
             part = buf[here, lower : lower + KEY_DIM].astype(F32)
@@ -202,7 +249,7 @@
         wide = query.astype(F32)
         if state is not None:
             out = out + dot((wide * jnp.exp(col)).astype(BF), state.astype(BF))
-        local_ref[here, :] = out
+        local_ref[here, :] = out.astype(BF)
         scaled_ref[here, :] = (wide * jnp.exp(col + base)).astype(BF)
         end = row[:, CHUNK - 1 : CHUNK]
         kept = (key.astype(F32) * jnp.exp(end - col)).astype(BF)
@@ -211,6 +258,7 @@
         base = base + end
     state_ref[0:KEY_DIM, :] = state.astype(BF)
     state_ref[KEY_DIM:, :] = split_total(base, (8, VALUE_DIM))
+    fetch(sems, (g_ref, g_hbm), (local_ref, local_hbm), (scaled_ref, scaled_hbm))
 
 
 def read_payload(ref):
@@ -232,8 +280,11 @@
     return state, gone
 
 
-def x_kernel(pos_ref, p0, p1, p2, p3, prefix_ref, gone_ref, state_ref):
-    pos = [pos_ref[i] for i in range(4)]
+NEAR = (0, 3, 1, 2)
+
+
+def x_kernel(me_ref, p0, p1, p2, p3, prefix_ref, gone_ref, state_ref):
+    pos = [(me_ref[0] + k) % 4 for k in NEAR]
     parts = [read_payload(p) for p in (p0, p1, p2, p3)]
     state, gone = before_me(pos, parts)
     prefix_ref[...] = state
@@ -251,17 +302,17 @@
 
 
 def gated_kernel(
-    pos_ref, core_ref, p0, p1, p2, p3, prefix_ref, gone_ref, local_ref, scaled_ref, gate_ref,
+    me_ref, p0, p1, p2, p3, prefix_ref, gone_ref, local_ref, scaled_ref, gate_ref,
     gain_ref, own_ref, twin_ref, buf,
 ):
-    pos = [pos_ref[i] for i in range(4)]
+    pos = [(me_ref[0] // 4 + k) % 4 for k in NEAR]
     parts = [read_payload(p) for p in (p0, p1, p2, p3)]
     state, _ = before_me(pos, parts)
     incoming = (prefix_ref[...] + gone_ref[0:1, :] * state).astype(BF)
-    retained = local_ref[...] + dot(scaled_ref[...], incoming)
+    retained = local_ref[...].astype(F32) + dot(scaled_ref[...], incoming)
     heads = normalised(retained, gain_ref[...])
     buf[...] = (silu(gate_ref[...].astype(F32)) * heads).astype(BF)
-    core = core_ref[0]
+    core = me_ref[1] % 2
     rows = own_ref.shape[0] // 4
     for y in range(4):
         there = slice(y * rows, (y + 1) * rows)
@@ -269,11 +320,12 @@
         twin_ref[there, :] = buf[pl.ds(pl.multiple_of((2 * y + 1 - core) * rows, rows), rows), :]
 
 
-def output_kernel(y_ref, own_ref, twin_ref, wo_ref, wt_ref, o0, o1, o2, o3, lhs, lht):
+def output_kernel(me_ref, own_ref, twin_ref, wo_ref, wt_ref, o0, o1, o2, o3, lhs, lht):
     rows = o0.shape[0]
     for k in range(4):
         here = slice(k * rows, (k + 1) * rows)
-        there = pl.ds(pl.multiple_of(y_ref[k] * rows, rows), rows)
+        y = (me_ref[1] // 2 + (0, 1, 3, 2)[k]) % 4
+        there = pl.ds(pl.multiple_of(y * rows, rows), rows)
         lhs[here, :] = own_ref[there, :]
         lht[here, :] = twin_ref[there, :]
     out = (dot(lhs[...], wo_ref[...]) + dot(lht[...], wt_ref[...])).astype(BF)
@@ -307,12 +359,15 @@
     return lax.all_to_all(x, axis, split_axis=0, concat_axis=0, tiled=True)
 
 
-def rotation(seg_rows):
+def rotation(positions):
     half = KEY_DIM // 2
-    position = (lax.axis_index("ep") * seg_rows + jnp.arange(seg_rows, dtype=jnp.int32)).astype(F32)
-    frequency = THETA ** (-jnp.arange(half, dtype=F32) / half)
-    angles = position[:, None] * frequency[None, :]
-    return jnp.concatenate([jnp.cos(angles), jnp.sin(angles)], axis=1)
+    frequency = THETA ** (-np.arange(half) / half)
+    angles = positions[:, None].astype(np.float64) * frequency[None, :]
+    cosine, sine = np.cos(angles), np.sin(angles)
+    return (
+        np.concatenate([cosine, cosine], axis=1).astype(np.float32),
+        np.concatenate([-sine, sine], axis=1).astype(np.float32),
+    )
 
 
 def local(
@@ -337,7 +392,6 @@
     rows, width = mixer_input.shape
     seg_rows = log_decay.shape[0]
     ep, tp = lax.axis_index("ep"), lax.axis_index("tp")
-    y, core = tp // 2, tp % 2
     n_ep, n_tp = lax.axis_size("ep"), lax.axis_size("tp")
     slots = n_ep * n_tp * CAP
 
@@ -352,7 +406,6 @@
     )
     from_below = y_shift(normed, 1)
     from_above = y_shift(normed, -1)
-    from_far = y_shift(normed, 2)
     twin = core_swap(normed)
 
     outgoing = run(
@@ -374,53 +427,82 @@
     twin_out = core_swap(output_weight)
     weights = (query_weight, key_weight, value_weight, gate_weight)
     cols = sum(w.shape[1] for w in weights)
-    turn = rotation(seg_rows)
-    decay = jnp.pad(log_decay.reshape(-1, CHUNK), ((0, 8 - seg_rows // CHUNK), (0, 0)))
-
+    cosine, sine = rotation(np.arange(seg_rows))
+    cosine_start, sine_start = rotation(np.arange(n_ep) * seg_rows)
+    me = jnp.stack([ep, tp]).astype(jnp.int32)
+    half = rows // 2
+    far_low = y_shift(from_below[:half], 1)
+    far_high = y_shift(from_above[half:], -1)
     below_twin, above_twin = core_swap(from_below), core_swap(from_above)
     early, joined = run(
         project_kernel,
         (shape((6 * rows, cols)), shape((width, cols))),
-        (normed, twin, from_below, below_twin, from_above, above_twin, *weights),
+        (
+            after(normed, me),
+            twin, from_below, below_twin, from_above, above_twin,
+            *weights,
+        ),
         flops=2 * 6 * rows * width * cols,
-        hbm=(6, 7, 8, 9),
-        scratch=(pltpu.VMEM((6 * rows, width), BF), sems(4)),
-    )
-    far_twin = core_swap(from_far)
-    away = jnp.array([0, 0, 3, 3, 1, 1, 2, 2], jnp.int32)
-    flip = jnp.array([0, 1] * 4, jnp.int32)
-    source = ((y + away) % 4) * 2 + (core + flip) % 2
+        hbm=range(10),
+        hbm_outs=(0, 1),
+        vmem=60 << 20,
+        scratch=(
+            pltpu.VMEM((6 * rows, width), BF),
+            *(pltpu.VMEM(w.shape, BF) for w in weights),
+            pltpu.VMEM((width, cols), BF),
+            pltpu.VMEM((6 * rows, cols), BF),
+            sems(10),
+            sems(1),
+        ),
+    )
+    low_twin, high_twin = core_swap(far_low), core_swap(far_high)
     gate, state, local_out, scaled = run(
         mixer_kernel,
         (
             shape((seg_rows, VALUE_DIM)),
             shape((KEY_DIM + 8, VALUE_DIM)),
-            shape((seg_rows, VALUE_DIM), F32),
+            shape((seg_rows, VALUE_DIM)),
             shape((seg_rows, KEY_DIM)),
         ),
-        (source, early, from_far, far_twin, joined, turn, decay),
+        (
+            me, early, far_low, far_high, low_twin, high_twin, joined,
+            cosine, sine, cosine_start, sine_start, log_decay.T,
+        ),
         scalars=1,
         flops=2 * 2 * rows * width * cols,
-        scratch=(pltpu.VMEM((2 * rows, width), BF), pltpu.VMEM((seg_rows, cols), BF)),
+        hbm=range(1, 12),
+        hbm_outs=(0, 2, 3),
+        vmem=60 << 20,
+        scratch=(
+            pltpu.VMEM((2 * rows, width), BF),
+            pltpu.VMEM((seg_rows, cols), BF),
+            pltpu.VMEM((6 * rows, cols), BF),
+            pltpu.VMEM((width, cols), BF),
+            pltpu.VMEM((seg_rows, KEY_DIM), F32),
+            pltpu.VMEM((seg_rows, KEY_DIM), F32),
+            pltpu.VMEM((n_ep, KEY_DIM), F32),
+            pltpu.VMEM((n_ep, KEY_DIM), F32),
+            pltpu.VMEM((1, seg_rows), F32),
+            pltpu.VMEM((8, CHUNK), F32),
+            pltpu.VMEM((seg_rows, VALUE_DIM), BF),
+            pltpu.VMEM((seg_rows, KEY_DIM), BF),
+            pltpu.VMEM((seg_rows, VALUE_DIM), BF),
+            sems(5),
+            sems(6),
+        ),
     )
 
     index = jnp.arange(slots, dtype=jnp.int32)
     deep = n_ep * CAP
-    to_tp = ((index % deep) * n_tp + index // deep)[:, None] == index[None, :]
-    source_row = (index // CAP % n_tp) * deep + index // (CAP * n_tp) * CAP + index % CAP
-    to_source = source_row[:, None] == index[None, :]
-    to_tp, to_source = to_tp.astype(BF), to_source.astype(BF)
+    to_tp = ((index % n_tp) * deep + index // n_tp)[None]
     turned = run(
-        permute_kernel,
+        turn_kernel,
         shape((slots, width)),
         (to_tp, after(staged, state).reshape(slots, width)),
         flops=2 * slots * slots * width,
     )
     tokens = exchange(turned.reshape(n_tp, deep, width), "tp").reshape(slots, width)
 
-    shifts = jnp.array([0, -1, 1, 2], jnp.int32)
-    x_pos = (ep % 4 + shifts + 4) % 4
-    z_pos = (ep // 4 + shifts + 4) % 4
     payloads = (state, x_shift(state, 1), x_shift(state, -1), x_shift(state, 2))
     prefix, gone, plane = run(
         x_kernel,
@@ -429,45 +511,47 @@
             shape((8, VALUE_DIM), F32),
             shape((KEY_DIM + 8, VALUE_DIM)),
         ),
-        (x_pos, *payloads),
+        (me, *payloads),
         scalars=1,
     )
     planes = (plane, z_shift(plane, 1), z_shift(plane, -1), z_shift(plane, 2))
     own_gated, twin_gated = run(
         gated_kernel,
         (shape((4 * rows, VALUE_DIM)), shape((4 * rows, VALUE_DIM))),
-        (z_pos, core.reshape(1), *planes, prefix, gone, local_out, scaled, gate, head_gain[None]),
-        scalars=2,
+        (me, *planes, prefix, gone, local_out, scaled, gate, head_gain[None]),
+        scalars=1,
         flops=2 * seg_rows * KEY_DIM * VALUE_DIM,
         scratch=(pltpu.VMEM((seg_rows, VALUE_DIM), BF),),
     )
     inner = expert_gate.shape[2]
-    tile, wide = 256, 512
-    params = pltpu.CompilerParams(
-        vmem_limit_bytes=60 << 20, dimension_semantics=("arbitrary",)
-    )
-    expand = pl.pallas_call(
-        hidden_kernel,
-        grid=(inner // tile,),
-        out_shape=shape((slots, inner)),
+    tile, wide = 512, 1024
+    first = inner // tile
+    experts = pl.pallas_call(
+        functools.partial(expert_kernel, first),
+        grid=(first + width // wide,),
+        out_shape=shape((n_ep * n_tp, CAP, width)),
         in_specs=[
             pl.BlockSpec((slots, width), lambda f: (0, 0)),
-            pl.BlockSpec((width, tile), lambda f: (0, f)),
-            pl.BlockSpec((width, tile), lambda f: (0, f)),
-            pl.BlockSpec((slots, slots), lambda f: (0, 0)),
+            pl.BlockSpec((width, tile), lambda f: (0, jnp.minimum(f, first - 1))),
+            pl.BlockSpec((width, tile), lambda f: (0, jnp.minimum(f, first - 1))),
+            pl.BlockSpec((inner, wide), lambda f: (0, jnp.maximum(f - first, 0))),
         ],
-        out_specs=pl.BlockSpec((slots, tile), lambda f: (0, f)),
-        compiler_params=params,
+        out_specs=pl.BlockSpec(
+            (n_ep * n_tp, CAP, wide), lambda f: (0, 0, jnp.maximum(f - first, 0))
+        ),
+        scratch_shapes=[pltpu.VMEM((slots, inner), BF)],
+        compiler_params=pltpu.CompilerParams(
+            vmem_limit_bytes=60 << 20, dimension_semantics=("arbitrary",)
+        ),
         cost_estimate=pl.CostEstimate(
-            flops=4 * slots * width * inner, bytes_accessed=4 * width * inner, transcendentals=0
+            flops=6 * slots * width * inner, bytes_accessed=6 * width * inner, transcendentals=0
         ),
     )
     other_gated = core_swap(twin_gated)
-    y_order = (y + jnp.array([0, 1, 3, 2], jnp.int32)) % 4
     kept, up, down, far = run(
         output_kernel,
         tuple(shape((rows, width)) for _ in range(4)),
-        (y_order, own_gated, other_gated, output_weight, twin_out),
+        (me, own_gated, other_gated, output_weight, twin_out),
         scalars=1,
         flops=2 * 4 * rows * 2 * VALUE_DIM * width,
         scratch=(pltpu.VMEM((4 * rows, VALUE_DIM), BF), pltpu.VMEM((4 * rows, VALUE_DIM), BF)),
@@ -475,26 +559,11 @@
     got_up = y_shift(up, 1)
     got_down = y_shift(down, -1)
     got_far = y_shift(far, 2)
-    hidden = expand(after(tokens, kept), expert_gate[0], expert_up[0], to_source)
+    results = experts(after(tokens, kept), expert_gate[0], expert_up[0], expert_down[0])
     mixer_output = run(sum_kernel, shape((rows, width)), (kept, got_up, got_down, got_far))
 
-    project_down = pl.pallas_call(
-        down_kernel,
-        grid=(width // wide,),
-        out_shape=shape((n_ep * n_tp, CAP, width)),
-        in_specs=[
-            pl.BlockSpec((slots, inner), lambda f: (0, 0)),
-            pl.BlockSpec((inner, wide), lambda f: (0, f)),
-        ],
-        out_specs=pl.BlockSpec((n_ep * n_tp, CAP, wide), lambda f: (0, 0, f)),
-        compiler_params=params,
-        cost_estimate=pl.CostEstimate(
-            flops=2 * slots * width * inner, bytes_accessed=2 * width * inner, transcendentals=0
-        ),
-    )
-    results = project_down(hidden, expert_down[0])
-    returned = exchange(results, ("ep", "tp"))
-    columns = jnp.stack([index // CAP, index % CAP])
+    returned = exchange(results, ("tp", "ep"))
+    columns = jnp.stack([index % deep // CAP * n_tp + index // deep, index % CAP])
     expert_output = run(
         combine_kernel,
         shape((rows, width)),

time: 163 us -> 165 us (1.012)
  waiting for transfers between devices: 55.4 us -> 68.1 us
  starting transfers between devices: 57.1 us -> 45.5 us
  other arithmetic: 3.82 us -> 0.71 us
  Pallas kernels: 39.5 us -> 42.5 us
    ppermute x6 -> x7, starting transfers between devices: 18.2 us -> 7.86 us  [core_swap(): return lax.ppermute(x, 'tp', [(t, t ^ 1) for t in range(8)])]
    ppermute x6 -> x7, waiting for transfers between devices: 48.1 us -> 57.8 us  [y_shift(): lax.ppermute(x, 'tp', [(t, (t // 2 + k) % 4 * 2 + t % 2) for t in range(8)])]
    pallas_call x10, Pallas kernels: 24.2 us -> 30.6 us  [run(): pl.pallas_call(kernel, out_shape=outs, in_specs=[SM if i < scalars else H...]
    pallas_call x2 -> x1, Pallas kernels: 15.3 us -> 11.9 us  [local(): experts(after(tokens, kept), expert_gate[0], expert_up[0], expert_down[0])]
    ppermute x3, waiting for transfers between devices: 3.39 us -> 5.34 us  [x_shift(): lax.ppermute(x, 'ep', [(e, e // 4 * 4 + (e + k) % 4) for e in range(16)])]
    slice x0 -> x2, local copies, waits for them, and re-layouts: none -> 1.93 us  [the longest x1 0.97 us: local(): far_low = y_shift(from_below[:half], 1)]
    cos x1 -> x0, other arithmetic: 1.88 us -> none  [rotation(): return jnp.concatenate([jnp.cos(angles), jnp.sin(angles)], axis=1)]
    ppermute x6 -> x7, starting transfers between devices: 8.97 us -> 10.2 us  [y_shift(): lax.ppermute(x, 'tp', [(t, (t // 2 + k) % 4 * 2 + t % 2) for t in range(8)])]
  transfers between devices with their start and end apart: 21 -> 23, of which waited for: 10 -> 10; matrix products, arithmetic and copies ran while one was open for 3% -> 2% of each run, Pallas kernels for 9% -> 13%
where the time goes in v1:
time: 165 us; the launch traced here: 164 us
  waiting for transfers between devices  68.1 us (41%)
  starting transfers between devices  45.5 us (28%)
  Pallas kernels  42.5 us (26%)
  local copies, waits for them, and re-layouts  6.71 us (4%)
    ppermute x7, waiting for transfers between devices, y_shift(): lax.ppermute(x, 'tp', [(t, (t // 2 + k) % 4 * 2 + t % 2) for t in range(8)])  57.8 us
    pallas_call x10, Pallas kernels, run(): pl.pallas_call(kernel, out_shape=outs, in_specs=[SM if i < scalars else H...  30.6 us
    all_to_all x3, starting transfers between devices, exchange(): return lax.all_to_all(x, axis, split_axis=0, concat_axis=0, tiled=True)  19.3 us
    pallas_call x1, Pallas kernels, local(): experts(after(tokens, kept), expert_gate[0], expert_up[0], expert_down[0])  11.9 us
    ppermute x7, starting transfers between devices, y_shift(): lax.ppermute(x, 'tp', [(t, (t // 2 + k) % 4 * 2 + t % 2) for t in range(8)])  10.2 us
    ppermute x7, starting transfers between devices, core_swap(): return lax.ppermute(x, 'tp', [(t, t ^ 1) for t in range(8)])  7.86 us
    ppermute x3, waiting for transfers between devices, x_shift(): lax.ppermute(x, 'ep', [(e, e // 4 * 4 + (e + k) % 4) for e in range(16)])  5.34 us
    unnamed x40, local copies, waits for them, and re-layouts  4.66 us
  transfers between devices with their start and end apart: 23, of which 10 were waited for; matrix products, arithmetic and copies ran while one was open for 2% of the time, Pallas kernels for 13%

profile of v1, /device:TPU:1, one launch (start us, length us, event | category | flops | bytes accessed | tf_op | source)
XLA Modules:
  0.0 164.4 jit_solution(1302627303679786163)
XLA Ops:
  0.6 2.2 %shard_map.212.refs_0_ = bf16[128,2048]{1,0:T(8,128)(2,1)} custom-call(bf16[128,2048]{1,0:T(8,128)(2,1)} %x_hbm.1, f32[1,2048]{1,0:T(1,128)} %bitcast.16), custom_call_target="tpu_custom_call" | custom-call | bytes 1056768 | tf_op jit(solution)/shard_map/pallas_call | solution.py:31
  2.8 3.1 %shard_map.219 = bf16[16,3,8,2048]{3,2,1,0:T(8,128)(2,1)} custom-call(bf16[128,2048]{1,0:T(8,128)(2,1)} %x_hbm.2, f32[1,2048]{1,0:T(1,128)} %bitcast.17, s32[2,128]{1,0:T(2,128)} %bitcast.18), custom_call_target="tpu_custom_call" | custom-call | flops 201326592 | bytes 2106368 | tf_op jit(solution)/shard_map/pallas_call | solution.py:31
  6.0 8.6 %all-to-all-start = ((bf16[16,3,8,2048]{3,2,1,0:T(8,128)(2,1)}), bf16[16,3,8,2048]{3,2,1,0:T(8,128)(2,1)S(1)}, u32[]{:S(2)}, u32[]{:S(2)}) async-start(bf16[16,3,8,2048]{3,2,1,0:T(8,128)(2,1)} %shard_map.219), calls=%async_computation | async-start | bytes 3145728 | tf_op jit(solution)/shard_map/all_to_all | solution.py:359
  15.9 1.5 collective-permute-start.3
  17.4 1.4 collective-permute-start
  18.8 9.7 %collective-permute-done.1.refs_2_ = bf16[128,2048]{1,0:T(8,128)(2,1)} collective-permute-done((bf16[128,2048]{1,0:T(8,128)(2,1)S(1)}, bf16[128,2048]{1,0:T(8,128)(2,1)}, u32[]{:S(2)}, u32[]{:S(2)}) %collective-permute-start.1) | collective-permute-done | bytes 524320 | tf_op jit(solution)/shard_map/ppermute | solution.py:347
  28.6 1.8 %collective-permute-start.2 = (bf16[128,2048]{1,0:T(8,128)(2,1)}, bf16[128,2048]{1,0:T(8,128)(2,1)}, u32[]{:S(2)}, u32[]{:S(2)}) collective-permute-start(bf16[128,2048]{1,0:T(8,128)(2,1)} %collective-permute-done.1.refs_2_), channel_id=1, source_target_pairs={{0,1},{1,0},{2,3},{3,2},{4,5},{5,4},{6,7},{7,6},{8,9},{9,8},{10,11... | collective-permute-start | bytes 1572872 | tf_op jit(solution)/shard_map/ppermute | solution.py:343
  31.3 1.4 collective-permute-start.5
  33.7 1.5 collective-permute-start.6
  35.2 4.9 %collective-permute-done.5.b0 = bf16[64,2048]{1,0:T(8,128)(2,1)S(1)} collective-permute-done((bf16[64,2048]{1,0:T(8,128)(2,1)S(1)}, bf16[64,2048]{1,0:T(8,128)(2,1)S(1)}, u32[]{:S(2)}, u32[]{:S(2)}) %collective-permute-start.5) | collective-permute-done | bytes 262176 | tf_op jit(solution)/shard_map/ppermute | solution.py:347
  43.1 6.5 %shard_map.213 = (bf16[768,768]{1,0:T(8,128)(2,1)}, bf16[2048,768]{1,0:T(8,128)(2,1)}) custom-call(bf16[128,2048]{1,0:T(8,128)(2,1)} %shard_map.212.refs_0_, bf16[128,2048]{1,0:T(8,128)(2,1)} %collective-permute-done.refs_1_, bf16[128,2048]{1,0:T(8,128)(2,1)} %collective-permute-done.1.refs_2_, bf16[128,2048]{1,0:T(8,128)(2,1)} %collective-permute-done.2.refs_3_, ...), custom_call_target="tpu_custom_call" | custom-call | flops 2415919104 | bytes 10616832 | tf_op jit(solution)/shard_map/pallas_call | solution.py:31
  50.5 8.4 %shard_map.214 = (bf16[1024,256]{1,0:T(8,128)(2,1)}, bf16[136,256]{1,0:T(8,128)(2,1)}, bf16[1024,256]{1,0:T(8,128)(2,1)}, bf16[1024,128]{1,0:T(8,128)(2,1)}) custom-call(s32[2]{0:T(128)} %pad_add_fusion.1.me_ref, bf16[768,768]{1,0:T(8,128)(2,1)} %get-tuple-element.22.early_hbm, bf16[64,2048]{1,0:T(8,128)(2,1)} %copy-done.12, bf16[64,2048]{1,0:T(8,128)(2,1)} %copy-done.13, ...), custom_call_target="tpu_custom_call" | custom-call | flops 805306368 | bytes 7823368 | tf_op jit(solution)/shard_map/pallas_call | solution.py:31
  58.9 2.2 %shard_map.220 = bf16[384,2048]{1,0:T(8,128)(2,1)} custom-call(s32[1,384]{1,0:T(1,128)S(1)} %fusion.2.index_ref, bf16[384,2048]{1,0:T(8,128)(2,1)S(1)} %bitcast.14), custom_call_target="tpu_custom_call" | custom-call | flops 603979776 | bytes 3147264 | tf_op jit(solution)/shard_map/pallas_call | solution.py:31
  61.1 4.5 %all-to-all-start.1 = ((bf16[8,48,2048]{2,1,0:T(8,128)(2,1)}), bf16[8,48,2048]{2,1,0:T(8,128)(2,1)}, u32[]{:S(2)}, u32[]{:S(2)}) async-start(bf16[8,48,2048]{2,1,0:T(8,128)(2,1)} %bitcast.8), calls=%async_computation.1 | async-start | bytes 3145728 | tf_op jit(solution)/shard_map/all_to_all | solution.py:359
  65.7 2.6 %collective-permute-start.10 = (bf16[136,256]{1,0:T(8,128)(2,1)S(1)}, bf16[136,256]{1,0:T(8,128)(2,1)S(1)}, u32[]{:S(2)}, u32[]{:S(2)}) collective-permute-start(bf16[136,256]{1,0:T(8,128)(2,1)S(1)} %copy-done.3), channel_id=1, source_target_pairs={{0,24},{8,0},{16,8},{24,16},{32,56},{40,32},{48,40},{56,48},{64,88... | collective-permute-start | bytes 208904 | tf_op jit(solution)/shard_map/ppermute | solution.py:351
  69.6 3.7 %collective-permute-done.11.p3 = bf16[136,256]{1,0:T(8,128)(2,1)S(1)} collective-permute-done((bf16[136,256]{1,0:T(8,128)(2,1)S(1)}, bf16[136,256]{1,0:T(8,128)(2,1)S(1)}, u32[]{:S(2)}, u32[]{:S(2)}) %collective-permute-start.11) | collective-permute-done | bytes 69664 | tf_op jit(solution)/shard_map/ppermute | solution.py:351
  73.3 1.4 collective-permute-done.9.p1
  75.5 1.4 collective-permute-start.12
  76.9 1.5 collective-permute-start.13
  78.4 1.5 collective-permute-start.14
  80.5 3.2 %collective-permute-done.14.p3 = bf16[136,256]{1,0:T(8,128)(2,1)S(1)} collective-permute-done((bf16[136,256]{1,0:T(8,128)(2,1)S(1)}, bf16[136,256]{1,0:T(8,128)(2,1)S(1)}, u32[]{:S(2)}, u32[]{:S(2)}) %collective-permute-start.14) | collective-permute-done | bytes 69664 | tf_op jit(solution)/shard_map/ppermute | solution.py:355
  83.7 1.5 shard_map.216
  85.2 2.2 %collective-permute-start.15 = (bf16[512,256]{1,0:T(8,128)(2,1)S(1)}, bf16[512,256]{1,0:T(8,128)(2,1)S(1)}, u32[]{:S(2)}, u32[]{:S(2)}) collective-permute-start(bf16[512,256]{1,0:T(8,128)(2,1)S(1)} %get-tuple-element.32), channel_id=1, source_target_pairs={{0,1},{1,0},{2,3},{3,2},{4,5},{5,4},{6,7},{7,6},{8,9},{9,8},{10,11... | collective-permute-start | bytes 786440 | tf_op jit(solution)/shard_map/ppermute | solution.py:343
  89.8 1.8 %shard_map.217 = (bf16[128,2048]{1,0:T(8,128)(2,1)S(1)}, bf16[128,2048]{1,0:T(8,128)(2,1)S(1)}, bf16[128,2048]{1,0:T(8,128)(2,1)S(1)}, bf16[128,2048]{1,0:T(8,128)(2,1)S(1)}) custom-call(s32[2]{0:T(128)S(1)} %copy-done.4, bf16[512,256]{1,0:T(8,128)(2,1)S(1)} %get-tuple-element.31.own_ref, bf16[512,256]{1,0:T(8,128)(2,1)S(1)} %collective-permute-done.15.twin_ref, ...), custom_call_target="tpu_custom_call" | custom-call | flops 1073741824 | bytes 4718600 | tf_op jit(solution)/shard_map/pallas_call | solution.py:31
  94.0 11.9 %shard_map.221 = bf16[128,3,2048]{2,1,0:T(4,128)(2,1)} custom-call(bf16[384,2048]{1,0:T(8,128)(2,1)} %bitcast.9.x_ref, bf16[2048,1024]{1,0:T(8,128)(2,1)} %bitcast.21, bf16[2048,1024]{1,0:T(8,128)(2,1)} %bitcast.22, bf16[1024,2048]{1,0:T(8,128)(2,1)} %bitcast.23), custom_call_target="tpu_custom_call" | custom-call | flops 4831838208 | bytes 12582912 | tf_op jit(solution)/shard_map/pallas_call | solution.py:562
  105.9 6.3 %all-to-all-start.2 = ((bf16[128,3,2048]{2,1,0:T(4,128)(2,1)}), bf16[128,3,2048]{2,1,0:T(4,128)(2,1)S(1)}, u32[]{:S(2)}, u32[]{:S(2)}) async-start(bf16[128,3,2048]{2,1,0:T(4,128)(2,1)} %shard_map.221), calls=%async_computation.2 | async-start | bytes 4194304 | tf_op jit(solution)/shard_map/all_to_all | solution.py:359
  112.2 1.4 collective-permute-start.17
  115.0 1.6 collective-permute-start.19
  117.0 31.8 %collective-permute-done.17.b = bf16[128,2048]{1,0:T(8,128)(2,1)S(1)} collective-permute-done((bf16[128,2048]{1,0:T(8,128)(2,1)}, bf16[128,2048]{1,0:T(8,128)(2,1)S(1)}, u32[]{:S(2)}, u32[]{:S(2)}) %collective-permute-start.17) | collective-permute-done | bytes 524320 | tf_op jit(solution)/shard_map/ppermute | solution.py:347
  148.9 11.3 %collective-permute-done.19.d = bf16[128,2048]{1,0:T(8,128)(2,1)} collective-permute-done((bf16[128,2048]{1,0:T(8,128)(2,1)}, bf16[128,2048]{1,0:T(8,128)(2,1)}, u32[]{:S(2)}, u32[]{:S(2)}) %collective-permute-start.19) | collective-permute-done | bytes 524320 | tf_op jit(solution)/shard_map/ppermute | solution.py:347
  160.2 2.2 %shard_map.218 = bf16[128,2048]{1,0:T(8,128)(2,1)} custom-call(bf16[128,2048]{1,0:T(8,128)(2,1)S(1)} %get-tuple-element.33.a, bf16[128,2048]{1,0:T(8,128)(2,1)S(1)} %collective-permute-done.17.b, bf16[128,2048]{1,0:T(8,128)(2,1)} %collective-permute-done.18.c, bf16[128,2048]{1,0:T(8,128)(2,1)} %collective-permute-done.19.d), custom_call_target="tpu_custom_call" | custom-call | bytes 2621440 | tf_op jit(solution)/shard_map/pallas_call | solution.py:31
  162.4 2.0 %shard_map.222 = bf16[128,2048]{1,0:T(8,128)(2,1)} custom-call(bf16[128,3,2048]{2,1,0:T(4,128)(2,1)S(1)} %all-to-all-done.2.rows_ref, s32[128,2]{1,0:T(8,128)S(1)} %copy.23.routes_ref, f32[128,1]{1,0:T(8,128)S(1)} %copy.24.group_ref, f32[128,2]{1,0:T(8,128)S(1)} %copy.25.pair_ref, s32[2,384]{1,0:T(2,128)S(1)} %pad_add_fusion.cols_ref), custom_call_target="tpu_custom_call" | custom-call | flops 402653184 | bytes 2102784 | tf_op jit(solution)/shard_map/pallas_call | solution.py:31
  (72 shorter events, 16.4 us)
Async XLA Ops:
  6.0 52.9 %all-to-all-start = ((bf16[16,3,8,2048]{3,2,1,0:T(8,128)(2,1)}), bf16[16,3,8,2048]{3,2,1,0:T(8,128)(2,1)S(1)}, u32[]{:S(2)}, u32[]{:S(2)}) async-start(bf16[16,3,8,2048]{3,2,1,0:T(8,128)(2,1)} %shard_map.219), calls=%async_computation | async-start | bytes 3145728 | tf_op jit(solution)/shard_map/all_to_all | solution.py:359
  14.5 14.0 %collective-permute-start.1 = (bf16[128,2048]{1,0:T(8,128)(2,1)S(1)}, bf16[128,2048]{1,0:T(8,128)(2,1)}, u32[]{:S(2)}, u32[]{:S(2)}) collective-permute-start(bf16[128,2048]{1,0:T(8,128)(2,1)S(1)} %copy-done.11), channel_id=1, source_target_pairs={{0,2},{1,3},{2,4},{3,5},{4,6},{5,7},{6,0},{7,1},{8,10},{9,11},{10,... | collective-permute-start | bytes 1572872 | tf_op jit(solution)/shard_map/ppermute | solution.py:347
  15.9 14.4 %collective-permute-start.3 = (bf16[128,2048]{1,0:T(8,128)(2,1)S(1)}, bf16[128,2048]{1,0:T(8,128)(2,1)}, u32[]{:S(2)}, u32[]{:S(2)}) collective-permute-start(bf16[128,2048]{1,0:T(8,128)(2,1)S(1)} %copy-done.11), channel_id=1, source_target_pairs={{0,6},{1,7},{2,0},{3,1},{4,2},{5,3},{6,4},{7,5},{8,14},{9,15},{10,... | collective-permute-start | bytes 1572872 | tf_op jit(solution)/shard_map/ppermute | solution.py:347
  17.4 25.7 %collective-permute-start = (bf16[128,2048]{1,0:T(8,128)(2,1)S(1)}, bf16[128,2048]{1,0:T(8,128)(2,1)}, u32[]{:S(2)}, u32[]{:S(2)}) collective-permute-start(bf16[128,2048]{1,0:T(8,128)(2,1)S(1)} %copy-done.11), channel_id=1, source_target_pairs={{0,1},{1,0},{2,3},{3,2},{4,5},{5,4},{6,7},{7,6},{8,9},{9,8},{10,11... | collective-permute-start | bytes 1572872 | tf_op jit(solution)/shard_map/ppermute | solution.py:343
  28.6 14.6 %collective-permute-start.2 = (bf16[128,2048]{1,0:T(8,128)(2,1)}, bf16[128,2048]{1,0:T(8,128)(2,1)}, u32[]{:S(2)}, u32[]{:S(2)}) collective-permute-start(bf16[128,2048]{1,0:T(8,128)(2,1)} %collective-permute-done.1.refs_2_), channel_id=1, source_target_pairs={{0,1},{1,0},{2,3},{3,2},{4,5},{5,4},{6,7},{7,6},{8,9},{9,8},{10,11... | collective-permute-start | bytes 1572872 | tf_op jit(solution)/shard_map/ppermute | solution.py:343
  30.3 12.8 %collective-permute-start.4 = (bf16[128,2048]{1,0:T(8,128)(2,1)}, bf16[128,2048]{1,0:T(8,128)(2,1)}, u32[]{:S(2)}, u32[]{:S(2)}) collective-permute-start(bf16[128,2048]{1,0:T(8,128)(2,1)} %collective-permute-done.3.refs_4_), channel_id=1, source_target_pairs={{0,1},{1,0},{2,3},{3,2},{4,5},{5,4},{6,7},{7,6},{8,9},{9,8},{10,11... | collective-permute-start | bytes 1572872 | tf_op jit(solution)/shard_map/ppermute | solution.py:343
  31.3 8.8 %collective-permute-start.5 = (bf16[64,2048]{1,0:T(8,128)(2,1)S(1)}, bf16[64,2048]{1,0:T(8,128)(2,1)S(1)}, u32[]{:S(2)}, u32[]{:S(2)}) collective-permute-start(bf16[64,2048]{1,0:T(8,128)(2,1)S(1)} %slice.8), channel_id=1, source_target_pairs={{0,2},{1,3},{2,4},{3,5},{4,6},{5,7},{6,0},{7,1},{8,10},{9,11},{10,... | collective-permute-start | bytes 786440 | tf_op jit(solution)/shard_map/ppermute | solution.py:347
  33.7 7.7 %collective-permute-start.6 = (bf16[64,2048]{1,0:T(8,128)(2,1)S(1)}, bf16[64,2048]{1,0:T(8,128)(2,1)S(1)}, u32[]{:S(2)}, u32[]{:S(2)}) collective-permute-start(bf16[64,2048]{1,0:T(8,128)(2,1)S(1)} %slice.9), channel_id=1, source_target_pairs={{0,6},{1,7},{2,0},{3,1},{4,2},{5,3},{6,4},{7,5},{8,14},{9,15},{10,... | collective-permute-start | bytes 786440 | tf_op jit(solution)/shard_map/ppermute | solution.py:347
  40.1 9.6 %copy-start.12 = (bf16[64,2048]{1,0:T(8,128)(2,1)}, bf16[64,2048]{1,0:T(8,128)(2,1)S(1)}, u32[]{:S(2)}) copy-start(bf16[64,2048]{1,0:T(8,128)(2,1)S(1)} %collective-permute-done.5.b0) | copy-start | bytes 786436
  40.1 9.6 %collective-permute-start.7 = (bf16[64,2048]{1,0:T(8,128)(2,1)S(1)}, bf16[64,2048]{1,0:T(8,128)(2,1)S(1)}, u32[]{:S(2)}, u32[]{:S(2)}) collective-permute-start(bf16[64,2048]{1,0:T(8,128)(2,1)S(1)} %collective-permute-done.5.b0), channel_id=1, source_target_pairs={{0,1},{1,0},{2,3},{3,2},{4,5},{5,4},{6,7},{7,6},{8,9},{9,8},{10,11... | collective-permute-start | bytes 786440 | tf_op jit(solution)/shard_map/ppermute | solution.py:343
  41.4 8.3 %collective-permute-start.8 = (bf16[64,2048]{1,0:T(8,128)(2,1)S(1)}, bf16[64,2048]{1,0:T(8,128)(2,1)S(1)}, u32[]{:S(2)}, u32[]{:S(2)}) collective-permute-start(bf16[64,2048]{1,0:T(8,128)(2,1)S(1)} %collective-permute-done.6.b1), channel_id=1, source_target_pairs={{0,1},{1,0},{2,3},{3,2},{4,5},{5,4},{6,7},{7,6},{8,9},{9,8},{10,11... | collective-permute-start | bytes 786440 | tf_op jit(solution)/shard_map/ppermute | solution.py:343
  61.1 13.7 %copy-start.4 = (s32[2]{0:T(128)S(1)}, s32[2]{0:T(128)}, u32[]{:S(2)}) copy-start(s32[2]{0:T(128)} %pad_add_fusion.1.me_ref) | copy-start | bytes 28
  61.1 22.6 %copy-start = (bf16[1024,256]{1,0:T(8,128)(2,1)S(1)}, bf16[1024,256]{1,0:T(8,128)(2,1)}, u32[]{:S(2)}) copy-start(bf16[1024,256]{1,0:T(8,128)(2,1)} %get-tuple-element.30.gate_ref) | copy-start | bytes 1572868
  61.1 22.6 %copy-start.1 = (bf16[1024,256]{1,0:T(8,128)(2,1)S(1)}, bf16[1024,256]{1,0:T(8,128)(2,1)}, u32[]{:S(2)}) copy-start(bf16[1024,256]{1,0:T(8,128)(2,1)} %get-tuple-element.28.local_ref) | copy-start | bytes 1572868
  61.1 22.6 %copy-start.2 = (bf16[1024,128]{1,0:T(8,128)(2,1)S(1)}, bf16[1024,128]{1,0:T(8,128)(2,1)}, u32[]{:S(2)}) copy-start(bf16[1024,128]{1,0:T(8,128)(2,1)} %get-tuple-element.29.scaled_ref) | copy-start | bytes 786436
  61.1 22.6 %copy-start.5 = (f32[256]{0:T(256)S(1)}, f32[256]{0:T(256)}, u32[]{:S(2)}) copy-start(f32[256]{0:T(256)} %param.28) | copy-start | bytes 3076
  61.1 33.0 %all-to-all-start.1 = ((bf16[8,48,2048]{2,1,0:T(8,128)(2,1)}), bf16[8,48,2048]{2,1,0:T(8,128)(2,1)}, u32[]{:S(2)}, u32[]{:S(2)}) async-start(bf16[8,48,2048]{2,1,0:T(8,128)(2,1)} %bitcast.8), calls=%async_computation.1 | async-start | bytes 3145728 | tf_op jit(solution)/shard_map/all_to_all | solution.py:359
  65.6 21.9 %collective-permute-start.16 = (bf16[256,2048]{1,0:T(8,128)(2,1)S(1)}, bf16[256,2048]{1,0:T(8,128)(2,1)S(1)}, u32[]{:S(2)}, u32[]{:S(2)}) collective-permute-start(bf16[256,2048]{1,0:T(8,128)(2,1)S(1)} %copy-done.6), channel_id=1, source_target_pairs={{0,1},{1,0},{2,3},{3,2},{4,5},{5,4},{6,7},{7,6},{8,9},{9,8},{10,11... | collective-permute-start | bytes 3145736 | tf_op jit(solution)/shard_map/ppermute | solution.py:343
  65.7 4.0 %collective-permute-start.10 = (bf16[136,256]{1,0:T(8,128)(2,1)S(1)}, bf16[136,256]{1,0:T(8,128)(2,1)S(1)}, u32[]{:S(2)}, u32[]{:S(2)}) collective-permute-start(bf16[136,256]{1,0:T(8,128)(2,1)S(1)} %copy-done.3), channel_id=1, source_target_pairs={{0,24},{8,0},{16,8},{24,16},{32,56},{40,32},{48,40},{56,48},{64,88... | collective-permute-start | bytes 208904 | tf_op jit(solution)/shard_map/ppermute | solution.py:351
  68.3 5.1 %collective-permute-start.11 = (bf16[136,256]{1,0:T(8,128)(2,1)S(1)}, bf16[136,256]{1,0:T(8,128)(2,1)S(1)}, u32[]{:S(2)}, u32[]{:S(2)}) collective-permute-start(bf16[136,256]{1,0:T(8,128)(2,1)S(1)} %copy-done.3), channel_id=1, source_target_pairs={{0,16},{8,24},{16,0},{24,8},{32,48},{40,56},{48,32},{56,40},{64,80... | collective-permute-start | bytes 208904 | tf_op jit(solution)/shard_map/ppermute | solution.py:351
  68.8 5.9 %collective-permute-start.9 = (bf16[136,256]{1,0:T(8,128)(2,1)S(1)}, bf16[136,256]{1,0:T(8,128)(2,1)S(1)}, u32[]{:S(2)}, u32[]{:S(2)}) collective-permute-start(bf16[136,256]{1,0:T(8,128)(2,1)S(1)} %copy-done.3), channel_id=1, source_target_pairs={{0,8},{8,16},{16,24},{24,0},{32,40},{40,48},{48,56},{56,32},{64,72... | collective-permute-start | bytes 208904 | tf_op jit(solution)/shard_map/ppermute | solution.py:351
  75.5 5.0 %collective-permute-start.12 = (bf16[136,256]{1,0:T(8,128)(2,1)S(1)}, bf16[136,256]{1,0:T(8,128)(2,1)S(1)}, u32[]{:S(2)}, u32[]{:S(2)}) collective-permute-start(bf16[136,256]{1,0:T(8,128)(2,1)S(1)} %get-tuple-element.25.p0), channel_id=1, source_target_pairs={{0,32},{8,40},{16,48},{24,56},{32,64},{40,72},{48,80},{56,88},{64,... | collective-permute-start | bytes 208904 | tf_op jit(solution)/shard_map/ppermute | solution.py:355
  76.9 3.6 %collective-permute-start.13 = (bf16[136,256]{1,0:T(8,128)(2,1)S(1)}, bf16[136,256]{1,0:T(8,128)(2,1)S(1)}, u32[]{:S(2)}, u32[]{:S(2)}) collective-permute-start(bf16[136,256]{1,0:T(8,128)(2,1)S(1)} %get-tuple-element.25.p0), channel_id=1, source_target_pairs={{0,96},{8,104},{16,112},{24,120},{32,0},{40,8},{48,16},{56,24},{64... | collective-permute-start | bytes 208904 | tf_op jit(solution)/shard_map/ppermute | solution.py:355
  78.4 5.3 %collective-permute-start.14 = (bf16[136,256]{1,0:T(8,128)(2,1)S(1)}, bf16[136,256]{1,0:T(8,128)(2,1)S(1)}, u32[]{:S(2)}, u32[]{:S(2)}) collective-permute-start(bf16[136,256]{1,0:T(8,128)(2,1)S(1)} %get-tuple-element.25.p0), channel_id=1, source_target_pairs={{0,64},{8,72},{16,80},{24,88},{32,96},{40,104},{48,112},{56,120},{... | collective-permute-start | bytes 208904 | tf_op jit(solution)/shard_map/ppermute | solution.py:355
  85.2 3.4 %collective-permute-start.15 = (bf16[512,256]{1,0:T(8,128)(2,1)S(1)}, bf16[512,256]{1,0:T(8,128)(2,1)S(1)}, u32[]{:S(2)}, u32[]{:S(2)}) collective-permute-start(bf16[512,256]{1,0:T(8,128)(2,1)S(1)} %get-tuple-element.32), channel_id=1, source_target_pairs={{0,1},{1,0},{2,3},{3,2},{4,5},{5,4},{6,7},{7,6},{8,9},{9,8},{10,11... | collective-permute-start | bytes 786440 | tf_op jit(solution)/shard_map/ppermute | solution.py:343
  105.9 10.7 %copy-start.16 = (s32[128,2]{0,1:T(2,128)S(1)}, s32[128,2]{0,1:T(2,128)}, u32[]{:S(2)}) copy-start(s32[128,2]{0,1:T(2,128)} %param.32) | copy-start | bytes 3076
  105.9 10.8 %copy-start.18 = (f32[128]{0:T(128)S(1)}, f32[128]{0:T(128)}, u32[]{:S(2)}) copy-start(f32[128]{0:T(128)} %param.33) | copy-start | bytes 1540
  105.9 10.9 %copy-start.17 = (f32[128,2]{0,1:T(2,128)S(1)}, f32[128,2]{0,1:T(2,128)}, u32[]{:S(2)}) copy-start(f32[128,2]{0,1:T(2,128)} %param.34) | copy-start | bytes 3076
  105.9 56.5 %all-to-all-start.2 = ((bf16[128,3,2048]{2,1,0:T(4,128)(2,1)}), bf16[128,3,2048]{2,1,0:T(4,128)(2,1)S(1)}, u32[]{:S(2)}, u32[]{:S(2)}) async-start(bf16[128,3,2048]{2,1,0:T(4,128)(2,1)} %shard_map.221), calls=%async_computation.2 | async-start | bytes 4194304 | tf_op jit(solution)/shard_map/all_to_all | solution.py:359
  112.2 36.6 %collective-permute-start.17 = (bf16[128,2048]{1,0:T(8,128)(2,1)}, bf16[128,2048]{1,0:T(8,128)(2,1)S(1)}, u32[]{:S(2)}, u32[]{:S(2)}) collective-permute-start(bf16[128,2048]{1,0:T(8,128)(2,1)} %copy-done.10), channel_id=1, source_target_pairs={{0,2},{1,3},{2,4},{3,5},{4,6},{5,7},{6,0},{7,1},{8,10},{9,11},{10,... | collective-permute-start | bytes 1572872 | tf_op jit(solution)/shard_map/ppermute | solution.py:347
  113.7 35.2 %collective-permute-start.18 = (bf16[128,2048]{1,0:T(8,128)(2,1)}, bf16[128,2048]{1,0:T(8,128)(2,1)}, u32[]{:S(2)}, u32[]{:S(2)}) collective-permute-start(bf16[128,2048]{1,0:T(8,128)(2,1)} %copy-done.9), channel_id=1, source_target_pairs={{0,6},{1,7},{2,0},{3,1},{4,2},{5,3},{6,4},{7,5},{8,14},{9,15},{10,... | collective-permute-start | bytes 1572872 | tf_op jit(solution)/shard_map/ppermute | solution.py:347
  115.0 45.1 %collective-permute-start.19 = (bf16[128,2048]{1,0:T(8,128)(2,1)}, bf16[128,2048]{1,0:T(8,128)(2,1)}, u32[]{:S(2)}, u32[]{:S(2)}) collective-permute-start(bf16[128,2048]{1,0:T(8,128)(2,1)} %copy-done.8), channel_id=1, source_target_pairs={{0,4},{1,5},{2,6},{3,7},{4,0},{5,1},{6,2},{7,3},{8,12},{9,13},{10,... | collective-permute-start | bytes 1572872 | tf_op jit(solution)/shard_map/ppermute | solution.py:347
  (10 other events, 31.1 us)

commit v2 on v1

--- a/solution.py
+++ b/solution.py
@@ -133,7 +133,7 @@
         o_ref[...] = dot(hidden[...], down_ref[...]).reshape(o_ref.shape).astype(BF)
 
 
-def combine_kernel(rows_ref, routes_ref, group_ref, pair_ref, cols_ref, o_ref):
+def mix_kernel(routes_ref, group_ref, pair_ref, cols_ref, high_ref, low_ref):
     tokens = routes_ref.shape[0]
     ids = cols_ref[0:1, :]
     slots = cols_ref[1:2, :].astype(F32)
@@ -148,9 +148,13 @@
     mix = jnp.where(first, weight[:, 0:1], 0.0) + jnp.where(second, weight[:, 1:2], 0.0)
     mix = jnp.where(rank == slots, mix, 0.0)
     high = mix.astype(BF)
-    low = (mix - high.astype(F32)).astype(BF)
-    rows = rows_ref[...].reshape(ids.shape[1], rows_ref.shape[2])
-    o_ref[...] = (dot(high, rows) + dot(low, rows)).astype(BF)
+    high_ref[...] = high
+    low_ref[...] = (mix - high.astype(F32)).astype(BF)
+
+
+def combine_kernel(rows_ref, high_ref, low_ref, o_ref):
+    rows = rows_ref[...].reshape(high_ref.shape[1], rows_ref.shape[2])
+    o_ref[...] = (dot(high_ref[...], rows) + dot(low_ref[...], rows)).astype(BF)
 
 
 def project_kernel(*refs):
@@ -188,50 +192,61 @@
 AWAY = (0, 3, 1, 2)
 
 
+def chunk_sums(decay_ref, steps_ref):
+    steps_ref[...] = jnp.zeros(steps_ref.shape, F32)
+    for i in range(decay_ref.shape[1] // CHUNK):
+        steps_ref[i : i + 1, :] = decay_ref[:, i * CHUNK : (i + 1) * CHUNK]
+    return prefix_sums(steps_ref[...])
+
+
 def mixer_kernel(
     me_ref, early_hbm, b0, b1, b2, b3, w_hbm, cos_hbm, sin_hbm, cos0, sin0, decay,
-    g_hbm, state_ref, local_hbm, scaled_hbm,
+    g_hbm, state_ref, q_hbm, k_hbm, v_hbm,
     lhs, buf, early_ref, w_ref, cos_ref, sin_ref, cos0_ref, sin0_ref, decay_ref, steps_ref,
-    local_ref, scaled_ref, g_ref, sems, late_sems,
+    q_ref, k_ref, v_ref, g_ref, kept_ref, sems, late_sems,
 ):
-    first = begin(sems, (w_hbm, w_ref), *rows_of(lhs, (b0, b1, b2, b3)))
     second = begin(
         late_sems,
+        (decay, decay_ref),
         (early_hbm, early_ref),
         (cos_hbm, cos_ref),
         (sin_hbm, sin_ref),
         (cos0, cos0_ref),
         (sin0, sin0_ref),
-        (decay, decay_ref),
-    )
+    )
+    first = begin(sems, (w_hbm, w_ref))
     segment, mine = me_ref[0], me_ref[1]
     y, core = mine // 2, mine % 2
     rows = 2 * b0.shape[0]
+    early = early_ref.shape[0] // rows
+
+    def placed(i, block):
+        owner = (y + AWAY[i // 2]) % 4 * 2 + (core + i) % 2
+        buf[pl.ds(pl.multiple_of(owner * rows, rows), rows), :] = block
+
+    finish(second)
+    sums = chunk_sums(decay_ref, steps_ref)
+    columns = sums.T
+    chunks = buf.shape[0] // CHUNK
+    ends = [sums[i : i + 1, CHUNK - 1 : CHUNK] for i in range(chunks)]
+    remain, total = [], jnp.zeros((1, 1), F32)
+    for i in reversed(range(chunks)):
+        remain.append(jnp.exp(total + ends[i] - columns[:, i : i + 1]))
+        total = total + ends[i]
+    remain = remain[::-1]
+    start_cos = cos0_ref[pl.ds(segment, 1), :]
+    start_sin = sin0_ref[pl.ds(segment, 1), :]
+    for i in range(early):
+        placed(i, early_ref[i * rows : (i + 1) * rows, :])
+    for block, there in rows_of(lhs, (b0, b1, b2, b3)):
+        there[...] = block[...]
     finish(first)
     late = dot(lhs[...], w_ref[...]).astype(BF)
-    finish(second)
-    early = early_ref.shape[0] // rows
-    for i in range(early + 2):
-        owner = (y + AWAY[i // 2]) % 4 * 2 + (core + i) % 2
-        here = pl.ds(pl.multiple_of(owner * rows, rows), rows)
-        if i < early:
-            buf[here, :] = early_ref[i * rows : (i + 1) * rows, :]
-        else:
-            buf[here, :] = late[(i - early) * rows : (i - early + 1) * rows, :]
+    for i in range(2):
+        placed(early + i, late[i * rows : (i + 1) * rows, :])
+    v_ref[...] = buf[:, 2 * KEY_DIM : 2 * KEY_DIM + VALUE_DIM]
     g_ref[...] = buf[:, 2 * KEY_DIM + VALUE_DIM :]
-
-    steps_ref[...] = jnp.zeros(steps_ref.shape, F32)
-    for i in range(buf.shape[0] // CHUNK):
-        steps_ref[i : i + 1, :] = decay_ref[:, i * CHUNK : (i + 1) * CHUNK]
-    sums = prefix_sums(steps_ref[...])
-    start_cos = cos0_ref[pl.ds(segment, 1), :]
-    start_sin = sin0_ref[pl.ds(segment, 1), :]
-    columns = sums.T
-    causal = lax.broadcasted_iota(jnp.int32, (CHUNK, CHUNK), 0) >= lax.broadcasted_iota(
-        jnp.int32, (CHUNK, CHUNK), 1
-    )
-    state, base = None, jnp.zeros((1, 1), F32)
-    for i in range(buf.shape[0] // CHUNK):
+    for i in range(chunks):
         here = slice(i * CHUNK, (i + 1) * CHUNK)
         cosine = cos_ref[here, :] * start_cos - sin_ref[here, :] * start_sin
         sine = sin_ref[here, :] * start_cos + cos_ref[here, :] * start_sin
@@ -240,8 +255,32 @@
             part = buf[here, lower : lower + KEY_DIM].astype(F32)
             return (part * cosine + pltpu.roll(part, KEY_DIM // 2, 1) * sine).astype(BF)
 
-        query, key = rotated(0), rotated(KEY_DIM)
-        value = buf[here, 2 * KEY_DIM : 2 * KEY_DIM + VALUE_DIM]
+        key = rotated(KEY_DIM)
+        k_ref[here, :] = key
+        kept_ref[here, :] = (key.astype(F32) * remain[i]).astype(BF)
+        q_ref[here, :] = rotated(0)
+    copies = begin(late_sems, (q_ref, q_hbm), (k_ref, k_hbm), (v_ref, v_hbm), (g_ref, g_hbm))
+    state_ref[0:KEY_DIM, :] = dot(kept_ref[...], v_ref[...], 0, 0).astype(BF)
+    state_ref[KEY_DIM:, :] = split_total(total, (8, VALUE_DIM))
+    finish(copies)
+
+
+def retain_kernel(
+    q_hbm, k_hbm, v_hbm, decay, local_ref, scaled_ref,
+    q_ref, k_ref, v_ref, decay_ref, steps_ref, sems,
+):
+    copies = begin(sems, (decay, decay_ref), (q_hbm, q_ref), (k_hbm, k_ref), (v_hbm, v_ref))
+    causal = lax.broadcasted_iota(jnp.int32, (CHUNK, CHUNK), 0) >= lax.broadcasted_iota(
+        jnp.int32, (CHUNK, CHUNK), 1
+    )
+    finish(copies)
+    sums = chunk_sums(decay_ref, steps_ref)
+    columns = sums.T
+    state, base = None, jnp.zeros((1, 1), F32)
+    chunks = q_ref.shape[0] // CHUNK
+    for i in range(chunks):
+        here = slice(i * CHUNK, (i + 1) * CHUNK)
+        query, key, value = q_ref[here, :], k_ref[here, :], v_ref[here, :]
         row, col = sums[i : i + 1, :], columns[:, i : i + 1]
         weight = jnp.where(causal, jnp.exp(jnp.minimum(col - row, 0.0)), 0.0)
         decayed = (dot(query, key, 1, 1) * weight).astype(BF)
@@ -252,13 +291,11 @@
         local_ref[here, :] = out.astype(BF)
         scaled_ref[here, :] = (wide * jnp.exp(col + base)).astype(BF)
         end = row[:, CHUNK - 1 : CHUNK]
-        kept = (key.astype(F32) * jnp.exp(end - col)).astype(BF)
-        update = dot(kept, value, 0, 0)
-        state = update if state is None else state * jnp.exp(end) + update
+        if i < chunks - 1:
+            kept = (key.astype(F32) * jnp.exp(end - col)).astype(BF)
+            update = dot(kept, value, 0, 0)
+            state = update if state is None else state * jnp.exp(end) + update
         base = base + end
-    state_ref[0:KEY_DIM, :] = state.astype(BF)
-    state_ref[KEY_DIM:, :] = split_total(base, (8, VALUE_DIM))
-    fetch(sems, (g_ref, g_hbm), (local_ref, local_hbm), (scaled_ref, scaled_hbm))
 
 
 def read_payload(ref):
@@ -394,6 +431,7 @@
     ep, tp = lax.axis_index("ep"), lax.axis_index("tp")
     n_ep, n_tp = lax.axis_size("ep"), lax.axis_size("tp")
     slots = n_ep * n_tp * CAP
+    me = jnp.stack([ep, tp]).astype(jnp.int32)
 
     sems = lambda n: pltpu.SemaphoreType.DMA((n,))
     normed = run(
@@ -411,7 +449,7 @@
     outgoing = run(
         dispatch_kernel,
         shape((n_ep, CAP, n_tp, width)),
-        (after(expert_input, normed), expert_gain[None], routes.T),
+        (after(expert_input, normed, me), expert_gain[None], routes.T),
         flops=2 * slots * rows * width,
         hbm=(0, 1, 2),
         vmem=60 << 20,
@@ -429,7 +467,6 @@
     cols = sum(w.shape[1] for w in weights)
     cosine, sine = rotation(np.arange(seg_rows))
     cosine_start, sine_start = rotation(np.arange(n_ep) * seg_rows)
-    me = jnp.stack([ep, tp]).astype(jnp.int32)
     half = rows // 2
     far_low = y_shift(from_below[:half], 1)
     far_high = y_shift(from_above[half:], -1)
@@ -438,7 +475,7 @@
         project_kernel,
         (shape((6 * rows, cols)), shape((width, cols))),
         (
-            after(normed, me),
+            normed,
             twin, from_below, below_twin, from_above, above_twin,
             *weights,
         ),
@@ -456,13 +493,14 @@
         ),
     )
     low_twin, high_twin = core_swap(far_low), core_swap(far_high)
-    gate, state, local_out, scaled = run(
+    gate, state, query, key, value = run(
         mixer_kernel,
         (
             shape((seg_rows, VALUE_DIM)),
             shape((KEY_DIM + 8, VALUE_DIM)),
+            shape((seg_rows, KEY_DIM)),
+            shape((seg_rows, KEY_DIM)),
             shape((seg_rows, VALUE_DIM)),
-            shape((seg_rows, KEY_DIM)),
         ),
         (
             me, early, far_low, far_high, low_twin, high_twin, joined,
@@ -470,8 +508,8 @@
         ),
         scalars=1,
         flops=2 * 2 * rows * width * cols,
-        hbm=range(1, 12),
-        hbm_outs=(0, 2, 3),
+        hbm=(1, 6, 7, 8, 9, 10, 11),
+        hbm_outs=(0, 2, 3, 4),
         vmem=60 << 20,
         scratch=(
             pltpu.VMEM((2 * rows, width), BF),
@@ -484,9 +522,11 @@
             pltpu.VMEM((n_ep, KEY_DIM), F32),
             pltpu.VMEM((1, seg_rows), F32),
             pltpu.VMEM((8, CHUNK), F32),
+            pltpu.VMEM((seg_rows, KEY_DIM), BF),
+            pltpu.VMEM((seg_rows, KEY_DIM), BF),
+            pltpu.VMEM((seg_rows, VALUE_DIM), BF),
             pltpu.VMEM((seg_rows, VALUE_DIM), BF),
             pltpu.VMEM((seg_rows, KEY_DIM), BF),
-            pltpu.VMEM((seg_rows, VALUE_DIM), BF),
             sems(5),
             sems(6),
         ),
@@ -515,6 +555,21 @@
         scalars=1,
     )
     planes = (plane, z_shift(plane, 1), z_shift(plane, -1), z_shift(plane, 2))
+    local_out, scaled = run(
+        retain_kernel,
+        (shape((seg_rows, VALUE_DIM)), shape((seg_rows, KEY_DIM))),
+        (query, key, value, log_decay.T),
+        flops=8 * seg_rows * CHUNK * VALUE_DIM,
+        hbm=range(4),
+        scratch=(
+            pltpu.VMEM((seg_rows, KEY_DIM), BF),
+            pltpu.VMEM((seg_rows, KEY_DIM), BF),
+            pltpu.VMEM((seg_rows, VALUE_DIM), BF),
+            pltpu.VMEM((1, seg_rows), F32),
+            pltpu.VMEM((8, CHUNK), F32),
+            sems(4),
+        ),
+    )
     own_gated, twin_gated = run(
         gated_kernel,
         (shape((4 * rows, VALUE_DIM)), shape((4 * rows, VALUE_DIM))),
@@ -564,10 +619,16 @@
 
     returned = exchange(results, ("tp", "ep"))
     columns = jnp.stack([index % deep // CAP * n_tp + index // deep, index % CAP])
+    high, low = run(
+        mix_kernel,
+        (shape((rows, slots)), shape((rows, slots))),
+        (routes, group_weight[:, None], pair_weight, columns),
+        flops=2 * slots * rows * rows,
+    )
     expert_output = run(
         combine_kernel,
         shape((rows, width)),
-        (returned, routes, group_weight[:, None], pair_weight, columns),
+        (returned, high, low),
         flops=4 * slots * rows * width,
     )
     return (mixer_output, expert_output)

time: 165 us -> 162 us (0.982)
    ppermute x3, waiting for transfers between devices: 3.81 us -> 1.76 us  [z_shift(): return lax.ppermute(x, 'ep', [(e, (e + 4 * k) % 16) for e in range(16)])]
    pallas_call x10 -> x12, Pallas kernels: 30.6 us -> 31.5 us  [run(): pl.pallas_call(kernel, out_shape=outs, in_specs=[SM if i < scalars else H...]
    unnamed x40 -> x50, local copies, waits for them, and re-layouts: 4.66 us -> 5.05 us
  transfers between devices with their start and end apart: 23 -> 23, of which waited for: 10 -> 9; matrix products, arithmetic and copies ran while one was open for 2% -> 0% of each run, Pallas kernels for 13% -> 14%
where the time goes in v2:
time: 162 us
  waiting for transfers between devices  66.8 us (41%)
  starting transfers between devices  44.6 us (28%)
  Pallas kernels  43.4 us (27%)
  local copies, waits for them, and re-layouts  5.2 us (3%)
    ppermute x7, waiting for transfers between devices, y_shift(): lax.ppermute(x, 'tp', [(t, (t // 2 + k) % 4 * 2 + t % 2) for t in range(8)])  58.4 us
    pallas_call x12, Pallas kernels, run(): pl.pallas_call(kernel, out_shape=outs, in_specs=[SM if i < scalars else H...  31.5 us
    all_to_all x3, starting transfers between devices, exchange(): return lax.all_to_all(x, axis, split_axis=0, concat_axis=0, tiled=True)  19.5 us
    pallas_call x1, Pallas kernels, local(): experts(after(tokens, kept), expert_gate[0], expert_up[0], expert_down[0])  11.9 us
    ppermute x7, starting transfers between devices, y_shift(): lax.ppermute(x, 'tp', [(t, (t // 2 + k) % 4 * 2 + t % 2) for t in range(8)])  10.1 us
    ppermute x7, starting transfers between devices, core_swap(): return lax.ppermute(x, 'tp', [(t, t ^ 1) for t in range(8)])  7.07 us
    ppermute x3, waiting for transfers between devices, x_shift(): lax.ppermute(x, 'ep', [(e, e // 4 * 4 + (e + k) % 4) for e in range(16)])  5.46 us
    unnamed x50, local copies, waits for them, and re-layouts  5.05 us
  transfers between devices with their start and end apart: 23, of which 9 were waited for; matrix products, arithmetic and copies ran while one was open for 0% of the time, Pallas kernels for 14%

profile of v2, /device:TPU:1, one launch (start us, length us, event | category | flops | bytes accessed | tf_op | source)
XLA Modules:
  0.0 161.7 jit_solution(9068981235920531169)
XLA Ops:
  0.6 2.2 %shard_map.212.refs_0_ = bf16[128,2048]{1,0:T(8,128)(2,1)} custom-call(bf16[128,2048]{1,0:T(8,128)(2,1)} %x_hbm.1, f32[1,2048]{1,0:T(1,128)} %bitcast.18), custom_call_target="tpu_custom_call" | custom-call | bytes 1056768 | tf_op jit(solution)/shard_map/pallas_call | solution.py:31
  3.5 3.1 %shard_map.220 = bf16[16,3,8,2048]{3,2,1,0:T(8,128)(2,1)} custom-call(bf16[128,2048]{1,0:T(8,128)(2,1)} %x_hbm.2, f32[1,2048]{1,0:T(1,128)} %bitcast.19, s32[2,128]{1,0:T(2,128)} %bitcast.20), custom_call_target="tpu_custom_call" | custom-call | flops 201326592 | bytes 2106368 | tf_op jit(solution)/shard_map/pallas_call | solution.py:31
  6.6 8.6 %all-to-all-start = ((bf16[16,3,8,2048]{3,2,1,0:T(8,128)(2,1)}), bf16[16,3,8,2048]{3,2,1,0:T(8,128)(2,1)S(1)}, u32[]{:S(2)}, u32[]{:S(2)}) async-start(bf16[16,3,8,2048]{3,2,1,0:T(8,128)(2,1)} %shard_map.220), calls=%async_computation | async-start | bytes 3145728 | tf_op jit(solution)/shard_map/all_to_all | solution.py:396
  15.2 1.4 collective-permute-start.1
  16.6 1.5 collective-permute-start.3
  18.1 1.4 collective-permute-start
  19.5 9.6 %collective-permute-done.1.refs_2_ = bf16[128,2048]{1,0:T(8,128)(2,1)S(1)} collective-permute-done((bf16[128,2048]{1,0:T(8,128)(2,1)S(1)}, bf16[128,2048]{1,0:T(8,128)(2,1)S(1)}, u32[]{:S(2)}, u32[]{:S(2)}) %collective-permute-start.1) | collective-permute-done | bytes 524320 | tf_op jit(solution)/shard_map/ppermute | solution.py:384
  29.1 1.8 %collective-permute-start.2 = (bf16[128,2048]{1,0:T(8,128)(2,1)S(1)}, bf16[128,2048]{1,0:T(8,128)(2,1)S(1)}, u32[]{:S(2)}, u32[]{:S(2)}) collective-permute-start(bf16[128,2048]{1,0:T(8,128)(2,1)S(1)} %collective-permute-done.1.refs_2_), channel_id=1, source_target_pairs={{0,1},{1,0},{2,3},{3,2},{4,5},{5,4},{6,7},{7,6},{8,9},{9,8},{10,11... | collective-permute-start | bytes 1572872 | tf_op jit(solution)/shard_map/ppermute | solution.py:380
  32.3 1.5 collective-permute-start.6
  33.9 5.9 %collective-permute-done.5.b0 = bf16[64,2048]{1,0:T(8,128)(2,1)S(1)} collective-permute-done((bf16[64,2048]{1,0:T(8,128)(2,1)S(1)}, bf16[64,2048]{1,0:T(8,128)(2,1)S(1)}, u32[]{:S(2)}, u32[]{:S(2)}) %collective-permute-start.5) | collective-permute-done | bytes 262176 | tf_op jit(solution)/shard_map/ppermute | solution.py:384
  42.8 6.5 %shard_map.213 = (bf16[768,768]{1,0:T(8,128)(2,1)}, bf16[2048,768]{1,0:T(8,128)(2,1)}) custom-call(bf16[128,2048]{1,0:T(8,128)(2,1)} %shard_map.212.refs_0_, bf16[128,2048]{1,0:T(8,128)(2,1)} %copy-done.22, bf16[128,2048]{1,0:T(8,128)(2,1)} %copy-done.17, bf16[128,2048]{1,0:T(8,128)(2,1)} %copy-done.23, bf16[128,2048]{1,0:T(8,128)(2,1)} %copy-done.18, ...), custom_call_target="tpu_custom_call" | custom-call | flops 2415919104 | bytes 10616832 | tf_op jit(solution)/shard_map/pallas_call | solution.py:31
  50.1 7.4 %shard_map.214 = (bf16[1024,256]{1,0:T(8,128)(2,1)}, bf16[136,256]{1,0:T(8,128)(2,1)}, bf16[1024,128]{1,0:T(8,128)(2,1)}, bf16[1024,128]{1,0:T(8,128)(2,1)}, bf16[1024,256]{1,0:T(8,128)(2,1)}) custom-call(s32[2]{0:T(128)} %pad_add_fusion.1.me_ref, bf16[768,768]{1,0:T(8,128)(2,1)} %get-tuple-element.25.early_hbm, bf16[64,2048]{1,0:T(8,128)(2,1)} %copy-done.13, ...), custom_call_target="tpu_custom_call" | custom-call | flops 805306368 | bytes 8085512 | tf_op jit(solution)/shard_map/pallas_call | solution.py:31
  57.5 2.2 %shard_map.221 = bf16[384,2048]{1,0:T(8,128)(2,1)} custom-call(s32[1,384]{1,0:T(1,128)S(1)} %fusion.2.index_ref, bf16[384,2048]{1,0:T(8,128)(2,1)S(1)} %bitcast.14), custom_call_target="tpu_custom_call" | custom-call | flops 603979776 | bytes 3147264 | tf_op jit(solution)/shard_map/pallas_call | solution.py:31
  59.8 4.7 %all-to-all-start.1 = ((bf16[8,48,2048]{2,1,0:T(8,128)(2,1)}), bf16[8,48,2048]{2,1,0:T(8,128)(2,1)}, u32[]{:S(2)}, u32[]{:S(2)}) async-start(bf16[8,48,2048]{2,1,0:T(8,128)(2,1)} %bitcast.8), calls=%async_computation.1 | async-start | bytes 3145728 | tf_op jit(solution)/shard_map/all_to_all | solution.py:396
  64.7 2.6 %collective-permute-start.10 = (bf16[136,256]{1,0:T(8,128)(2,1)S(1)}, bf16[136,256]{1,0:T(8,128)(2,1)S(1)}, u32[]{:S(2)}, u32[]{:S(2)}) collective-permute-start(bf16[136,256]{1,0:T(8,128)(2,1)S(1)} %copy-done.1), channel_id=1, source_target_pairs={{0,24},{8,0},{16,8},{24,16},{32,56},{40,32},{48,40},{56,48},{64,88... | collective-permute-start | bytes 208904 | tf_op jit(solution)/shard_map/ppermute | solution.py:388
  68.6 3.7 %collective-permute-done.11.p3 = bf16[136,256]{1,0:T(8,128)(2,1)S(1)} collective-permute-done((bf16[136,256]{1,0:T(8,128)(2,1)S(1)}, bf16[136,256]{1,0:T(8,128)(2,1)S(1)}, u32[]{:S(2)}, u32[]{:S(2)}) %collective-permute-start.11) | collective-permute-done | bytes 69664 | tf_op jit(solution)/shard_map/ppermute | solution.py:388
  72.3 1.6 collective-permute-done.9.p1
  75.9 1.5 collective-permute-start.13
  77.3 1.5 collective-permute-start.14
  78.8 1.9 %shard_map.216 = (bf16[1024,256]{1,0:T(8,128)(2,1)S(1)}, bf16[1024,128]{1,0:T(8,128)(2,1)S(1)}) custom-call(bf16[1024,128]{1,0:T(8,128)(2,1)S(1)} %copy-done.10, bf16[1024,128]{1,0:T(8,128)(2,1)S(1)} %copy-done.11, bf16[1024,256]{1,0:T(8,128)(2,1)S(1)} %copy-done.6, f32[1,1024]{1,0:T(1,128)S(1)} %bitcast.16), custom_call_target="tpu_custom_call" | custom-call | flops 536870912 | bytes 1839104 | tf_op jit(solution)/shard_map/pallas_call | solution.py:31
  80.8 1.8 %collective-permute-done.14.p3 = bf16[136,256]{1,0:T(8,128)(2,1)S(1)} collective-permute-done((bf16[136,256]{1,0:T(8,128)(2,1)S(1)}, bf16[136,256]{1,0:T(8,128)(2,1)S(1)}, u32[]{:S(2)}, u32[]{:S(2)}) %collective-permute-start.14) | collective-permute-done | bytes 69664 | tf_op jit(solution)/shard_map/ppermute | solution.py:392
  82.5 1.5 shard_map.217
  84.0 2.2 %collective-permute-start.15 = (bf16[512,256]{1,0:T(8,128)(2,1)S(1)}, bf16[512,256]{1,0:T(8,128)(2,1)S(1)}, u32[]{:S(2)}, u32[]{:S(2)}) collective-permute-start(bf16[512,256]{1,0:T(8,128)(2,1)S(1)} %get-tuple-element.38), channel_id=1, source_target_pairs={{0,1},{1,0},{2,3},{3,2},{4,5},{5,4},{6,7},{7,6},{8,9},{9,8},{10,11... | collective-permute-start | bytes 786440 | tf_op jit(solution)/shard_map/ppermute | solution.py:380
  87.4 1.8 %shard_map.218 = (bf16[128,2048]{1,0:T(8,128)(2,1)S(1)}, bf16[128,2048]{1,0:T(8,128)(2,1)S(1)}, bf16[128,2048]{1,0:T(8,128)(2,1)S(1)}, bf16[128,2048]{1,0:T(8,128)(2,1)S(1)}) custom-call(s32[2]{0:T(128)S(1)} %copy-done.2, bf16[512,256]{1,0:T(8,128)(2,1)S(1)} %get-tuple-element.37.own_ref, bf16[512,256]{1,0:T(8,128)(2,1)S(1)} %collective-permute-done.15.twin_ref, ...), custom_call_target="tpu_custom_call" | custom-call | flops 1073741824 | bytes 4718600 | tf_op jit(solution)/shard_map/pallas_call | solution.py:31
  91.6 11.9 %shard_map.222 = bf16[128,3,2048]{2,1,0:T(4,128)(2,1)} custom-call(bf16[384,2048]{1,0:T(8,128)(2,1)} %bitcast.9.x_ref, bf16[2048,1024]{1,0:T(8,128)(2,1)} %bitcast.22, bf16[2048,1024]{1,0:T(8,128)(2,1)} %bitcast.23, bf16[1024,2048]{1,0:T(8,128)(2,1)} %bitcast.24), custom_call_target="tpu_custom_call" | custom-call | flops 4831838208 | bytes 12582912 | tf_op jit(solution)/shard_map/pallas_call | solution.py:617
  103.5 6.2 %all-to-all-start.2 = ((bf16[128,3,2048]{2,1,0:T(4,128)(2,1)}), bf16[128,3,2048]{2,1,0:T(4,128)(2,1)S(1)}, u32[]{:S(2)}, u32[]{:S(2)}) async-start(bf16[128,3,2048]{2,1,0:T(4,128)(2,1)} %shard_map.222), calls=%async_computation.2 | async-start | bytes 4194304 | tf_op jit(solution)/shard_map/all_to_all | solution.py:396
  109.7 1.4 collective-permute-start.17
  112.5 1.6 %collective-permute-start.19 = (bf16[128,2048]{1,0:T(8,128)(2,1)}, bf16[128,2048]{1,0:T(8,128)(2,1)}, u32[]{:S(2)}, u32[]{:S(2)}) collective-permute-start(bf16[128,2048]{1,0:T(8,128)(2,1)} %copy-done.7), channel_id=1, source_target_pairs={{0,4},{1,5},{2,6},{3,7},{4,0},{5,1},{6,2},{7,3},{8,12},{9,13},{10,... | collective-permute-start | bytes 1572872 | tf_op jit(solution)/shard_map/ppermute | solution.py:384
  114.8 31.5 %collective-permute-done.17.b = bf16[128,2048]{1,0:T(8,128)(2,1)S(1)} collective-permute-done((bf16[128,2048]{1,0:T(8,128)(2,1)}, bf16[128,2048]{1,0:T(8,128)(2,1)S(1)}, u32[]{:S(2)}, u32[]{:S(2)}) %collective-permute-start.17) | collective-permute-done | bytes 524320 | tf_op jit(solution)/shard_map/ppermute | solution.py:384
  146.3 11.3 %collective-permute-done.19.d = bf16[128,2048]{1,0:T(8,128)(2,1)} collective-permute-done((bf16[128,2048]{1,0:T(8,128)(2,1)}, bf16[128,2048]{1,0:T(8,128)(2,1)}, u32[]{:S(2)}, u32[]{:S(2)}) %collective-permute-start.19) | collective-permute-done | bytes 524320 | tf_op jit(solution)/shard_map/ppermute | solution.py:384
  157.7 2.2 %shard_map.219 = bf16[128,2048]{1,0:T(8,128)(2,1)} custom-call(bf16[128,2048]{1,0:T(8,128)(2,1)S(1)} %get-tuple-element.39.a, bf16[128,2048]{1,0:T(8,128)(2,1)S(1)} %collective-permute-done.17.b, bf16[128,2048]{1,0:T(8,128)(2,1)} %collective-permute-done.18.c, bf16[128,2048]{1,0:T(8,128)(2,1)} %collective-permute-done.19.d), custom_call_target="tpu_custom_call" | custom-call | bytes 2621440 | tf_op jit(solution)/shard_map/pallas_call | solution.py:31
  159.9 1.8 %shard_map.224 = bf16[128,2048]{1,0:T(8,128)(2,1)} custom-call(bf16[128,3,2048]{2,1,0:T(4,128)(2,1)S(1)} %all-to-all-done.2.rows_ref, bf16[128,384]{1,0:T(8,128)(2,1)S(1)} %get-tuple-element.46.high_ref, bf16[128,384]{1,0:T(8,128)(2,1)S(1)} %get-tuple-element.47.low_ref), custom_call_target="tpu_custom_call" | custom-call | flops 402653184 | bytes 2293760 | tf_op jit(solution)/shard_map/pallas_call | solution.py:31
  (84 shorter events, 15.0 us)
Async XLA Ops:
  6.6 50.9 %all-to-all-start = ((bf16[16,3,8,2048]{3,2,1,0:T(8,128)(2,1)}), bf16[16,3,8,2048]{3,2,1,0:T(8,128)(2,1)S(1)}, u32[]{:S(2)}, u32[]{:S(2)}) async-start(bf16[16,3,8,2048]{3,2,1,0:T(8,128)(2,1)} %shard_map.220), calls=%async_computation | async-start | bytes 3145728 | tf_op jit(solution)/shard_map/all_to_all | solution.py:396
  15.2 13.9 %collective-permute-start.1 = (bf16[128,2048]{1,0:T(8,128)(2,1)S(1)}, bf16[128,2048]{1,0:T(8,128)(2,1)S(1)}, u32[]{:S(2)}, u32[]{:S(2)}) collective-permute-start(bf16[128,2048]{1,0:T(8,128)(2,1)S(1)} %copy-done.12), channel_id=1, source_target_pairs={{0,2},{1,3},{2,4},{3,5},{4,6},{5,7},{6,0},{7,1},{8,10},{9,11},{10,... | collective-permute-start | bytes 1572872 | tf_op jit(solution)/shard_map/ppermute | solution.py:384
  16.6 14.3 %collective-permute-start.3 = (bf16[128,2048]{1,0:T(8,128)(2,1)S(1)}, bf16[128,2048]{1,0:T(8,128)(2,1)S(1)}, u32[]{:S(2)}, u32[]{:S(2)}) collective-permute-start(bf16[128,2048]{1,0:T(8,128)(2,1)S(1)} %copy-done.12), channel_id=1, source_target_pairs={{0,6},{1,7},{2,0},{3,1},{4,2},{5,3},{6,4},{7,5},{8,14},{9,15},{10,... | collective-permute-start | bytes 1572872 | tf_op jit(solution)/shard_map/ppermute | solution.py:384
  18.1 23.0 %collective-permute-start = (bf16[128,2048]{1,0:T(8,128)(2,1)S(1)}, bf16[128,2048]{1,0:T(8,128)(2,1)S(1)}, u32[]{:S(2)}, u32[]{:S(2)}) collective-permute-start(bf16[128,2048]{1,0:T(8,128)(2,1)S(1)} %copy-done.12), channel_id=1, source_target_pairs={{0,1},{1,0},{2,3},{3,2},{4,5},{5,4},{6,7},{7,6},{8,9},{9,8},{10,11... | collective-permute-start | bytes 1572872 | tf_op jit(solution)/shard_map/ppermute | solution.py:380
  29.1 13.7 %copy-start.17 = (bf16[128,2048]{1,0:T(8,128)(2,1)}, bf16[128,2048]{1,0:T(8,128)(2,1)S(1)}, u32[]{:S(2)}) copy-start(bf16[128,2048]{1,0:T(8,128)(2,1)S(1)} %collective-permute-done.1.refs_2_) | copy-start | bytes 1572868
  29.1 12.0 %collective-permute-start.2 = (bf16[128,2048]{1,0:T(8,128)(2,1)S(1)}, bf16[128,2048]{1,0:T(8,128)(2,1)S(1)}, u32[]{:S(2)}, u32[]{:S(2)}) collective-permute-start(bf16[128,2048]{1,0:T(8,128)(2,1)S(1)} %collective-permute-done.1.refs_2_), channel_id=1, source_target_pairs={{0,1},{1,0},{2,3},{3,2},{4,5},{5,4},{6,7},{7,6},{8,9},{9,8},{10,11... | collective-permute-start | bytes 1572872 | tf_op jit(solution)/shard_map/ppermute | solution.py:380
  30.9 11.9 %collective-permute-start.4 = (bf16[128,2048]{1,0:T(8,128)(2,1)S(1)}, bf16[128,2048]{1,0:T(8,128)(2,1)}, u32[]{:S(2)}, u32[]{:S(2)}) collective-permute-start(bf16[128,2048]{1,0:T(8,128)(2,1)S(1)} %collective-permute-done.3.refs_4_), channel_id=1, source_target_pairs={{0,1},{1,0},{2,3},{3,2},{4,5},{5,4},{6,7},{7,6},{8,9},{9,8},{10,11... | collective-permute-start | bytes 1572872 | tf_op jit(solution)/shard_map/ppermute | solution.py:380
  31.0 8.7 %collective-permute-start.5 = (bf16[64,2048]{1,0:T(8,128)(2,1)S(1)}, bf16[64,2048]{1,0:T(8,128)(2,1)S(1)}, u32[]{:S(2)}, u32[]{:S(2)}) collective-permute-start(bf16[64,2048]{1,0:T(8,128)(2,1)S(1)} %slice.8), channel_id=1, source_target_pairs={{0,2},{1,3},{2,4},{3,5},{4,6},{5,7},{6,0},{7,1},{8,10},{9,11},{10,... | collective-permute-start | bytes 786440 | tf_op jit(solution)/shard_map/ppermute | solution.py:384
  32.3 8.7 %collective-permute-start.6 = (bf16[64,2048]{1,0:T(8,128)(2,1)S(1)}, bf16[64,2048]{1,0:T(8,128)(2,1)S(1)}, u32[]{:S(2)}, u32[]{:S(2)}) collective-permute-start(bf16[64,2048]{1,0:T(8,128)(2,1)S(1)} %slice.9), channel_id=1, source_target_pairs={{0,6},{1,7},{2,0},{3,1},{4,2},{5,3},{6,4},{7,5},{8,14},{9,15},{10,... | collective-permute-start | bytes 786440 | tf_op jit(solution)/shard_map/ppermute | solution.py:384
  39.7 9.6 %collective-permute-start.7 = (bf16[64,2048]{1,0:T(8,128)(2,1)S(1)}, bf16[64,2048]{1,0:T(8,128)(2,1)S(1)}, u32[]{:S(2)}, u32[]{:S(2)}) collective-permute-start(bf16[64,2048]{1,0:T(8,128)(2,1)S(1)} %collective-permute-done.5.b0), channel_id=1, source_target_pairs={{0,1},{1,0},{2,3},{3,2},{4,5},{5,4},{6,7},{7,6},{8,9},{9,8},{10,11... | collective-permute-start | bytes 786440 | tf_op jit(solution)/shard_map/ppermute | solution.py:380
  41.0 8.4 %collective-permute-start.8 = (bf16[64,2048]{1,0:T(8,128)(2,1)S(1)}, bf16[64,2048]{1,0:T(8,128)(2,1)S(1)}, u32[]{:S(2)}, u32[]{:S(2)}) collective-permute-start(bf16[64,2048]{1,0:T(8,128)(2,1)S(1)} %collective-permute-done.6.b1), channel_id=1, source_target_pairs={{0,1},{1,0},{2,3},{3,2},{4,5},{5,4},{6,7},{7,6},{8,9},{9,8},{10,11... | collective-permute-start | bytes 786440 | tf_op jit(solution)/shard_map/ppermute | solution.py:380
  59.7 14.2 %copy-start.2 = (s32[2]{0:T(128)S(1)}, s32[2]{0:T(128)}, u32[]{:S(2)}) copy-start(s32[2]{0:T(128)} %pad_add_fusion.1.me_ref) | copy-start | bytes 28
  59.7 19.1 %copy-start.3 = (f32[1024,1]{0,1:T(1,128)S(1)}, f32[1024,1]{0,1:T(1,128)}, u32[]{:S(2)}) copy-start(f32[1024,1]{0,1:T(1,128)} %param.22) | copy-start | bytes 12292
  59.7 19.1 %copy-start.6 = (bf16[1024,256]{1,0:T(8,128)(2,1)S(1)}, bf16[1024,256]{1,0:T(8,128)(2,1)}, u32[]{:S(2)}) copy-start(bf16[1024,256]{1,0:T(8,128)(2,1)} %get-tuple-element.33.v_hbm) | copy-start | bytes 1572868
  59.7 19.1 %copy-start.10 = (bf16[1024,128]{1,0:T(8,128)(2,1)S(1)}, bf16[1024,128]{1,0:T(8,128)(2,1)}, u32[]{:S(2)}) copy-start(bf16[1024,128]{1,0:T(8,128)(2,1)} %get-tuple-element.31.q_hbm) | copy-start | bytes 786436
  59.7 19.1 %copy-start.11 = (bf16[1024,128]{1,0:T(8,128)(2,1)S(1)}, bf16[1024,128]{1,0:T(8,128)(2,1)}, u32[]{:S(2)}) copy-start(bf16[1024,128]{1,0:T(8,128)(2,1)} %get-tuple-element.32.k_hbm) | copy-start | bytes 786436
  59.7 22.8 %copy-start = (bf16[1024,256]{1,0:T(8,128)(2,1)S(1)}, bf16[1024,256]{1,0:T(8,128)(2,1)}, u32[]{:S(2)}) copy-start(bf16[1024,256]{1,0:T(8,128)(2,1)} %get-tuple-element.36.gate_ref) | copy-start | bytes 1572868
  59.7 22.8 %copy-start.4 = (f32[256]{0:T(256)S(1)}, f32[256]{0:T(256)}, u32[]{:S(2)}) copy-start(f32[256]{0:T(256)} %param.28) | copy-start | bytes 3076
  59.8 31.9 %all-to-all-start.1 = ((bf16[8,48,2048]{2,1,0:T(8,128)(2,1)}), bf16[8,48,2048]{2,1,0:T(8,128)(2,1)}, u32[]{:S(2)}, u32[]{:S(2)}) async-start(bf16[8,48,2048]{2,1,0:T(8,128)(2,1)} %bitcast.8), calls=%async_computation.1 | async-start | bytes 3145728 | tf_op jit(solution)/shard_map/all_to_all | solution.py:396
  64.5 21.8 %collective-permute-start.16 = (bf16[256,2048]{1,0:T(8,128)(2,1)S(1)}, bf16[256,2048]{1,0:T(8,128)(2,1)S(1)}, u32[]{:S(2)}, u32[]{:S(2)}) collective-permute-start(bf16[256,2048]{1,0:T(8,128)(2,1)S(1)} %copy-done.5), channel_id=1, source_target_pairs={{0,1},{1,0},{2,3},{3,2},{4,5},{5,4},{6,7},{7,6},{8,9},{9,8},{10,11... | collective-permute-start | bytes 3145736 | tf_op jit(solution)/shard_map/ppermute | solution.py:380
  64.7 3.9 %collective-permute-start.10 = (bf16[136,256]{1,0:T(8,128)(2,1)S(1)}, bf16[136,256]{1,0:T(8,128)(2,1)S(1)}, u32[]{:S(2)}, u32[]{:S(2)}) collective-permute-start(bf16[136,256]{1,0:T(8,128)(2,1)S(1)} %copy-done.1), channel_id=1, source_target_pairs={{0,24},{8,0},{16,8},{24,16},{32,56},{40,32},{48,40},{56,48},{64,88... | collective-permute-start | bytes 208904 | tf_op jit(solution)/shard_map/ppermute | solution.py:388
  67.3 5.1 %collective-permute-start.11 = (bf16[136,256]{1,0:T(8,128)(2,1)S(1)}, bf16[136,256]{1,0:T(8,128)(2,1)S(1)}, u32[]{:S(2)}, u32[]{:S(2)}) collective-permute-start(bf16[136,256]{1,0:T(8,128)(2,1)S(1)} %copy-done.1), channel_id=1, source_target_pairs={{0,16},{8,24},{16,0},{24,8},{32,48},{40,56},{48,32},{56,40},{64,80... | collective-permute-start | bytes 208904 | tf_op jit(solution)/shard_map/ppermute | solution.py:388
  67.8 6.1 %collective-permute-start.9 = (bf16[136,256]{1,0:T(8,128)(2,1)S(1)}, bf16[136,256]{1,0:T(8,128)(2,1)S(1)}, u32[]{:S(2)}, u32[]{:S(2)}) collective-permute-start(bf16[136,256]{1,0:T(8,128)(2,1)S(1)} %copy-done.1), channel_id=1, source_target_pairs={{0,8},{8,16},{16,24},{24,0},{32,40},{40,48},{48,56},{56,32},{64,72... | collective-permute-start | bytes 208904 | tf_op jit(solution)/shard_map/ppermute | solution.py:388
  74.6 6.1 %collective-permute-start.12 = (bf16[136,256]{1,0:T(8,128)(2,1)S(1)}, bf16[136,256]{1,0:T(8,128)(2,1)S(1)}, u32[]{:S(2)}, u32[]{:S(2)}) collective-permute-start(bf16[136,256]{1,0:T(8,128)(2,1)S(1)} %get-tuple-element.28.p0), channel_id=1, source_target_pairs={{0,32},{8,40},{16,48},{24,56},{32,64},{40,72},{48,80},{56,88},{64,... | collective-permute-start | bytes 208904 | tf_op jit(solution)/shard_map/ppermute | solution.py:392
  75.9 4.9 %collective-permute-start.13 = (bf16[136,256]{1,0:T(8,128)(2,1)S(1)}, bf16[136,256]{1,0:T(8,128)(2,1)S(1)}, u32[]{:S(2)}, u32[]{:S(2)}) collective-permute-start(bf16[136,256]{1,0:T(8,128)(2,1)S(1)} %get-tuple-element.28.p0), channel_id=1, source_target_pairs={{0,96},{8,104},{16,112},{24,120},{32,0},{40,8},{48,16},{56,24},{64... | collective-permute-start | bytes 208904 | tf_op jit(solution)/shard_map/ppermute | solution.py:392
  77.3 5.2 %collective-permute-start.14 = (bf16[136,256]{1,0:T(8,128)(2,1)S(1)}, bf16[136,256]{1,0:T(8,128)(2,1)S(1)}, u32[]{:S(2)}, u32[]{:S(2)}) collective-permute-start(bf16[136,256]{1,0:T(8,128)(2,1)S(1)} %get-tuple-element.28.p0), channel_id=1, source_target_pairs={{0,64},{8,72},{16,80},{24,88},{32,96},{40,104},{48,112},{56,120},{... | collective-permute-start | bytes 208904 | tf_op jit(solution)/shard_map/ppermute | solution.py:392
  84.0 3.4 %collective-permute-start.15 = (bf16[512,256]{1,0:T(8,128)(2,1)S(1)}, bf16[512,256]{1,0:T(8,128)(2,1)S(1)}, u32[]{:S(2)}, u32[]{:S(2)}) collective-permute-start(bf16[512,256]{1,0:T(8,128)(2,1)S(1)} %get-tuple-element.38), channel_id=1, source_target_pairs={{0,1},{1,0},{2,3},{3,2},{4,5},{5,4},{6,7},{7,6},{8,9},{9,8},{10,11... | collective-permute-start | bytes 786440 | tf_op jit(solution)/shard_map/ppermute | solution.py:380
  103.5 10.9 %copy-start.20 = (f32[128,2]{0,1:T(2,128)S(1)}, f32[128,2]{0,1:T(2,128)}, u32[]{:S(2)}) copy-start(f32[128,2]{0,1:T(2,128)} %param.34) | copy-start | bytes 3076
  103.5 56.4 %all-to-all-start.2 = ((bf16[128,3,2048]{2,1,0:T(4,128)(2,1)}), bf16[128,3,2048]{2,1,0:T(4,128)(2,1)S(1)}, u32[]{:S(2)}, u32[]{:S(2)}) async-start(bf16[128,3,2048]{2,1,0:T(4,128)(2,1)} %shard_map.222), calls=%async_computation.2 | async-start | bytes 4194304 | tf_op jit(solution)/shard_map/all_to_all | solution.py:396
  109.7 36.6 %collective-permute-start.17 = (bf16[128,2048]{1,0:T(8,128)(2,1)}, bf16[128,2048]{1,0:T(8,128)(2,1)S(1)}, u32[]{:S(2)}, u32[]{:S(2)}) collective-permute-start(bf16[128,2048]{1,0:T(8,128)(2,1)} %copy-done.9), channel_id=1, source_target_pairs={{0,2},{1,3},{2,4},{3,5},{4,6},{5,7},{6,0},{7,1},{8,10},{9,11},{10,... | collective-permute-start | bytes 1572872 | tf_op jit(solution)/shard_map/ppermute | solution.py:384
  111.2 35.2 %collective-permute-start.18 = (bf16[128,2048]{1,0:T(8,128)(2,1)}, bf16[128,2048]{1,0:T(8,128)(2,1)}, u32[]{:S(2)}, u32[]{:S(2)}) collective-permute-start(bf16[128,2048]{1,0:T(8,128)(2,1)} %copy-done.8), channel_id=1, source_target_pairs={{0,6},{1,7},{2,0},{3,1},{4,2},{5,3},{6,4},{7,5},{8,14},{9,15},{10,... | collective-permute-start | bytes 1572872 | tf_op jit(solution)/shard_map/ppermute | solution.py:384
  112.5 45.1 %collective-permute-start.19 = (bf16[128,2048]{1,0:T(8,128)(2,1)}, bf16[128,2048]{1,0:T(8,128)(2,1)}, u32[]{:S(2)}, u32[]{:S(2)}) collective-permute-start(bf16[128,2048]{1,0:T(8,128)(2,1)} %copy-done.7), channel_id=1, source_target_pairs={{0,4},{1,5},{2,6},{3,7},{4,0},{5,1},{6,2},{7,3},{8,12},{9,13},{10,... | collective-permute-start | bytes 1572872 | tf_op jit(solution)/shard_map/ppermute | solution.py:384
  (15 other events, 73.4 us)

commit v3 on v2

--- a/solution.py
+++ b/solution.py
@@ -288,7 +288,7 @@
         wide = query.astype(F32)
         if state is not None:
             out = out + dot((wide * jnp.exp(col)).astype(BF), state.astype(BF))
-        local_ref[here, :] = out.astype(BF)
+        local_ref[here, :] = out
         scaled_ref[here, :] = (wide * jnp.exp(col + base)).astype(BF)
         end = row[:, CHUNK - 1 : CHUNK]
         if i < chunks - 1:
@@ -346,7 +346,7 @@
     parts = [read_payload(p) for p in (p0, p1, p2, p3)]
     state, _ = before_me(pos, parts)
     incoming = (prefix_ref[...] + gone_ref[0:1, :] * state).astype(BF)
-    retained = local_ref[...].astype(F32) + dot(scaled_ref[...], incoming)
+    retained = local_ref[...] + dot(scaled_ref[...], incoming)
     heads = normalised(retained, gain_ref[...])
     buf[...] = (silu(gate_ref[...].astype(F32)) * heads).astype(BF)
     core = me_ref[1] % 2
@@ -557,7 +557,7 @@
     planes = (plane, z_shift(plane, 1), z_shift(plane, -1), z_shift(plane, 2))
     local_out, scaled = run(
         retain_kernel,
-        (shape((seg_rows, VALUE_DIM)), shape((seg_rows, KEY_DIM))),
+        (shape((seg_rows, VALUE_DIM), F32), shape((seg_rows, KEY_DIM))),
         (query, key, value, log_decay.T),
         flops=8 * seg_rows * CHUNK * VALUE_DIM,
         hbm=range(4),
@@ -611,9 +611,9 @@
         flops=2 * 4 * rows * 2 * VALUE_DIM * width,
         scratch=(pltpu.VMEM((4 * rows, VALUE_DIM), BF), pltpu.VMEM((4 * rows, VALUE_DIM), BF)),
     )
+    got_far = y_shift(far, 2)
     got_up = y_shift(up, 1)
     got_down = y_shift(down, -1)
-    got_far = y_shift(far, 2)
     results = experts(after(tokens, kept), expert_gate[0], expert_up[0], expert_down[0])
     mixer_output = run(sum_kernel, shape((rows, width)), (kept, got_up, got_down, got_far))
 

time: 162 us -> 162 us (level)
  no operation moved by 1% of the time
where the time goes in v3:
time: 162 us
  waiting for transfers between devices  66.8 us (41%)
  starting transfers between devices  44.6 us (28%)
  Pallas kernels  43.3 us (27%)
  local copies, waits for them, and re-layouts  5.2 us (3%)
    ppermute x7, waiting for transfers between devices, y_shift(): lax.ppermute(x, 'tp', [(t, (t // 2 + k) % 4 * 2 + t % 2) for t in range(8)])  58.4 us
    pallas_call x12, Pallas kernels, run(): pl.pallas_call(kernel, out_shape=outs, in_specs=[SM if i < scalars else H...  31.5 us
    all_to_all x3, starting transfers between devices, exchange(): return lax.all_to_all(x, axis, split_axis=0, concat_axis=0, tiled=True)  19.5 us
    pallas_call x1, Pallas kernels, local(): experts(after(tokens, kept), expert_gate[0], expert_up[0], expert_down[0])  11.9 us
    ppermute x7, starting transfers between devices, y_shift(): lax.ppermute(x, 'tp', [(t, (t // 2 + k) % 4 * 2 + t % 2) for t in range(8)])  10.1 us
    ppermute x7, starting transfers between devices, core_swap(): return lax.ppermute(x, 'tp', [(t, t ^ 1) for t in range(8)])  7.07 us
    ppermute x3, waiting for transfers between devices, x_shift(): lax.ppermute(x, 'ep', [(e, e // 4 * 4 + (e + k) % 4) for e in range(16)])  5.46 us
    unnamed x50, local copies, waits for them, and re-layouts  5.05 us
  transfers between devices with their start and end apart: 23, of which 9 were waited for; matrix products, arithmetic and copies ran while one was open for 0% of the time, Pallas kernels for 14%

profile of v3, /device:TPU:1, one launch (start us, length us, event | category | flops | bytes accessed | tf_op | source)
XLA Modules:
  0.0 161.6 jit_solution(4910140953547564499)
XLA Ops:
  0.6 2.2 %shard_map.212.refs_0_ = bf16[128,2048]{1,0:T(8,128)(2,1)} custom-call(bf16[128,2048]{1,0:T(8,128)(2,1)} %x_hbm.1, f32[1,2048]{1,0:T(1,128)} %bitcast.18), custom_call_target="tpu_custom_call" | custom-call | bytes 1056768 | tf_op jit(solution)/shard_map/pallas_call | solution.py:31
  3.5 3.1 %shard_map.220 = bf16[16,3,8,2048]{3,2,1,0:T(8,128)(2,1)} custom-call(bf16[128,2048]{1,0:T(8,128)(2,1)} %x_hbm.2, f32[1,2048]{1,0:T(1,128)} %bitcast.19, s32[2,128]{1,0:T(2,128)} %bitcast.20), custom_call_target="tpu_custom_call" | custom-call | flops 201326592 | bytes 2106368 | tf_op jit(solution)/shard_map/pallas_call | solution.py:31
  6.6 8.6 %all-to-all-start = ((bf16[16,3,8,2048]{3,2,1,0:T(8,128)(2,1)}), bf16[16,3,8,2048]{3,2,1,0:T(8,128)(2,1)S(1)}, u32[]{:S(2)}, u32[]{:S(2)}) async-start(bf16[16,3,8,2048]{3,2,1,0:T(8,128)(2,1)} %shard_map.220), calls=%async_computation | async-start | bytes 3145728 | tf_op jit(solution)/shard_map/all_to_all | solution.py:396
  15.2 1.4 collective-permute-start.1
  16.6 1.5 collective-permute-start.3
  18.1 1.4 collective-permute-start
  19.5 9.6 %collective-permute-done.1.refs_2_ = bf16[128,2048]{1,0:T(8,128)(2,1)S(1)} collective-permute-done((bf16[128,2048]{1,0:T(8,128)(2,1)S(1)}, bf16[128,2048]{1,0:T(8,128)(2,1)S(1)}, u32[]{:S(2)}, u32[]{:S(2)}) %collective-permute-start.1) | collective-permute-done | bytes 524320 | tf_op jit(solution)/shard_map/ppermute | solution.py:384
  29.1 1.8 %collective-permute-start.2 = (bf16[128,2048]{1,0:T(8,128)(2,1)S(1)}, bf16[128,2048]{1,0:T(8,128)(2,1)S(1)}, u32[]{:S(2)}, u32[]{:S(2)}) collective-permute-start(bf16[128,2048]{1,0:T(8,128)(2,1)S(1)} %collective-permute-done.1.refs_2_), channel_id=1, source_target_pairs={{0,1},{1,0},{2,3},{3,2},{4,5},{5,4},{6,7},{7,6},{8,9},{9,8},{10,11... | collective-permute-start | bytes 1572872 | tf_op jit(solution)/shard_map/ppermute | solution.py:380
  32.3 1.5 collective-permute-start.6
  33.9 5.9 %collective-permute-done.5.b0 = bf16[64,2048]{1,0:T(8,128)(2,1)S(1)} collective-permute-done((bf16[64,2048]{1,0:T(8,128)(2,1)S(1)}, bf16[64,2048]{1,0:T(8,128)(2,1)S(1)}, u32[]{:S(2)}, u32[]{:S(2)}) %collective-permute-start.5) | collective-permute-done | bytes 262176 | tf_op jit(solution)/shard_map/ppermute | solution.py:384
  42.8 6.5 %shard_map.213 = (bf16[768,768]{1,0:T(8,128)(2,1)}, bf16[2048,768]{1,0:T(8,128)(2,1)}) custom-call(bf16[128,2048]{1,0:T(8,128)(2,1)} %shard_map.212.refs_0_, bf16[128,2048]{1,0:T(8,128)(2,1)} %copy-done.22, bf16[128,2048]{1,0:T(8,128)(2,1)} %copy-done.17, bf16[128,2048]{1,0:T(8,128)(2,1)} %copy-done.23, bf16[128,2048]{1,0:T(8,128)(2,1)} %copy-done.18, ...), custom_call_target="tpu_custom_call" | custom-call | flops 2415919104 | bytes 10616832 | tf_op jit(solution)/shard_map/pallas_call | solution.py:31
  50.1 7.4 %shard_map.214 = (bf16[1024,256]{1,0:T(8,128)(2,1)}, bf16[136,256]{1,0:T(8,128)(2,1)}, bf16[1024,128]{1,0:T(8,128)(2,1)}, bf16[1024,128]{1,0:T(8,128)(2,1)}, bf16[1024,256]{1,0:T(8,128)(2,1)}) custom-call(s32[2]{0:T(128)} %pad_add_fusion.1.me_ref, bf16[768,768]{1,0:T(8,128)(2,1)} %get-tuple-element.25.early_hbm, bf16[64,2048]{1,0:T(8,128)(2,1)} %copy-done.13, ...), custom_call_target="tpu_custom_call" | custom-call | flops 805306368 | bytes 8085512 | tf_op jit(solution)/shard_map/pallas_call | solution.py:31
  57.5 2.2 %shard_map.221 = bf16[384,2048]{1,0:T(8,128)(2,1)} custom-call(s32[1,384]{1,0:T(1,128)S(1)} %fusion.2.index_ref, bf16[384,2048]{1,0:T(8,128)(2,1)S(1)} %bitcast.14), custom_call_target="tpu_custom_call" | custom-call | flops 603979776 | bytes 3147264 | tf_op jit(solution)/shard_map/pallas_call | solution.py:31
  59.8 4.7 %all-to-all-start.1 = ((bf16[8,48,2048]{2,1,0:T(8,128)(2,1)}), bf16[8,48,2048]{2,1,0:T(8,128)(2,1)}, u32[]{:S(2)}, u32[]{:S(2)}) async-start(bf16[8,48,2048]{2,1,0:T(8,128)(2,1)} %bitcast.8), calls=%async_computation.1 | async-start | bytes 3145728 | tf_op jit(solution)/shard_map/all_to_all | solution.py:396
  64.7 2.6 %collective-permute-start.10 = (bf16[136,256]{1,0:T(8,128)(2,1)S(1)}, bf16[136,256]{1,0:T(8,128)(2,1)S(1)}, u32[]{:S(2)}, u32[]{:S(2)}) collective-permute-start(bf16[136,256]{1,0:T(8,128)(2,1)S(1)} %copy-done.1), channel_id=1, source_target_pairs={{0,24},{8,0},{16,8},{24,16},{32,56},{40,32},{48,40},{56,48},{64,88... | collective-permute-start | bytes 208904 | tf_op jit(solution)/shard_map/ppermute | solution.py:388
  68.6 3.7 %collective-permute-done.11.p3 = bf16[136,256]{1,0:T(8,128)(2,1)S(1)} collective-permute-done((bf16[136,256]{1,0:T(8,128)(2,1)S(1)}, bf16[136,256]{1,0:T(8,128)(2,1)S(1)}, u32[]{:S(2)}, u32[]{:S(2)}) %collective-permute-start.11) | collective-permute-done | bytes 69664 | tf_op jit(solution)/shard_map/ppermute | solution.py:388
  72.3 1.6 collective-permute-done.9.p1
  75.9 1.5 collective-permute-start.13
  77.3 1.5 collective-permute-start.14
  78.8 1.8 %shard_map.216 = (f32[1024,256]{1,0:T(8,128)S(1)}, bf16[1024,128]{1,0:T(8,128)(2,1)S(1)}) custom-call(bf16[1024,128]{1,0:T(8,128)(2,1)S(1)} %copy-done.10, bf16[1024,128]{1,0:T(8,128)(2,1)S(1)} %copy-done.11, bf16[1024,256]{1,0:T(8,128)(2,1)S(1)} %copy-done.6, f32[1,1024]{1,0:T(1,128)S(1)} %bitcast.16), custom_call_target="tpu_custom_call" | custom-call | flops 536870912 | bytes 2363392 | tf_op jit(solution)/shard_map/pallas_call | solution.py:31
  80.7 1.8 %collective-permute-done.14.p3 = bf16[136,256]{1,0:T(8,128)(2,1)S(1)} collective-permute-done((bf16[136,256]{1,0:T(8,128)(2,1)S(1)}, bf16[136,256]{1,0:T(8,128)(2,1)S(1)}, u32[]{:S(2)}, u32[]{:S(2)}) %collective-permute-start.14) | collective-permute-done | bytes 69664 | tf_op jit(solution)/shard_map/ppermute | solution.py:392
  82.5 1.5 shard_map.217
  84.0 2.2 %collective-permute-start.15 = (bf16[512,256]{1,0:T(8,128)(2,1)S(1)}, bf16[512,256]{1,0:T(8,128)(2,1)S(1)}, u32[]{:S(2)}, u32[]{:S(2)}) collective-permute-start(bf16[512,256]{1,0:T(8,128)(2,1)S(1)} %get-tuple-element.38), channel_id=1, source_target_pairs={{0,1},{1,0},{2,3},{3,2},{4,5},{5,4},{6,7},{7,6},{8,9},{9,8},{10,11... | collective-permute-start | bytes 786440 | tf_op jit(solution)/shard_map/ppermute | solution.py:380
  87.4 1.8 %shard_map.218 = (bf16[128,2048]{1,0:T(8,128)(2,1)S(1)}, bf16[128,2048]{1,0:T(8,128)(2,1)S(1)}, bf16[128,2048]{1,0:T(8,128)(2,1)S(1)}, bf16[128,2048]{1,0:T(8,128)(2,1)S(1)}) custom-call(s32[2]{0:T(128)S(1)} %copy-done.2, bf16[512,256]{1,0:T(8,128)(2,1)S(1)} %get-tuple-element.37.own_ref, bf16[512,256]{1,0:T(8,128)(2,1)S(1)} %collective-permute-done.15.twin_ref, ...), custom_call_target="tpu_custom_call" | custom-call | flops 1073741824 | bytes 4718600 | tf_op jit(solution)/shard_map/pallas_call | solution.py:31
  91.6 11.9 %shard_map.222 = bf16[128,3,2048]{2,1,0:T(4,128)(2,1)} custom-call(bf16[384,2048]{1,0:T(8,128)(2,1)} %bitcast.9.x_ref, bf16[2048,1024]{1,0:T(8,128)(2,1)} %bitcast.22, bf16[2048,1024]{1,0:T(8,128)(2,1)} %bitcast.23, bf16[1024,2048]{1,0:T(8,128)(2,1)} %bitcast.24), custom_call_target="tpu_custom_call" | custom-call | flops 4831838208 | bytes 12582912 | tf_op jit(solution)/shard_map/pallas_call | solution.py:617
  103.5 6.2 %all-to-all-start.2 = ((bf16[128,3,2048]{2,1,0:T(4,128)(2,1)}), bf16[128,3,2048]{2,1,0:T(4,128)(2,1)S(1)}, u32[]{:S(2)}, u32[]{:S(2)}) async-start(bf16[128,3,2048]{2,1,0:T(4,128)(2,1)} %shard_map.222), calls=%async_computation.2 | async-start | bytes 4194304 | tf_op jit(solution)/shard_map/all_to_all | solution.py:396
  109.7 1.4 collective-permute-start.17
  112.5 1.6 %collective-permute-start.19 = (bf16[128,2048]{1,0:T(8,128)(2,1)}, bf16[128,2048]{1,0:T(8,128)(2,1)}, u32[]{:S(2)}, u32[]{:S(2)}) collective-permute-start(bf16[128,2048]{1,0:T(8,128)(2,1)} %copy-done.7), channel_id=1, source_target_pairs={{0,4},{1,5},{2,6},{3,7},{4,0},{5,1},{6,2},{7,3},{8,12},{9,13},{10,... | collective-permute-start | bytes 1572872 | tf_op jit(solution)/shard_map/ppermute | solution.py:384
  114.8 31.5 %collective-permute-done.17.b = bf16[128,2048]{1,0:T(8,128)(2,1)S(1)} collective-permute-done((bf16[128,2048]{1,0:T(8,128)(2,1)}, bf16[128,2048]{1,0:T(8,128)(2,1)S(1)}, u32[]{:S(2)}, u32[]{:S(2)}) %collective-permute-start.17) | collective-permute-done | bytes 524320 | tf_op jit(solution)/shard_map/ppermute | solution.py:384
  146.3 11.3 %collective-permute-done.19.d = bf16[128,2048]{1,0:T(8,128)(2,1)} collective-permute-done((bf16[128,2048]{1,0:T(8,128)(2,1)}, bf16[128,2048]{1,0:T(8,128)(2,1)}, u32[]{:S(2)}, u32[]{:S(2)}) %collective-permute-start.19) | collective-permute-done | bytes 524320 | tf_op jit(solution)/shard_map/ppermute | solution.py:384
  157.6 2.2 %shard_map.219 = bf16[128,2048]{1,0:T(8,128)(2,1)} custom-call(bf16[128,2048]{1,0:T(8,128)(2,1)S(1)} %get-tuple-element.39.a, bf16[128,2048]{1,0:T(8,128)(2,1)S(1)} %collective-permute-done.17.b, bf16[128,2048]{1,0:T(8,128)(2,1)} %collective-permute-done.18.c, bf16[128,2048]{1,0:T(8,128)(2,1)} %collective-permute-done.19.d), custom_call_target="tpu_custom_call" | custom-call | bytes 2621440 | tf_op jit(solution)/shard_map/pallas_call | solution.py:31
  159.9 1.7 %shard_map.224 = bf16[128,2048]{1,0:T(8,128)(2,1)} custom-call(bf16[128,3,2048]{2,1,0:T(4,128)(2,1)S(1)} %all-to-all-done.2.rows_ref, bf16[128,384]{1,0:T(8,128)(2,1)S(1)} %get-tuple-element.46.high_ref, bf16[128,384]{1,0:T(8,128)(2,1)S(1)} %get-tuple-element.47.low_ref), custom_call_target="tpu_custom_call" | custom-call | flops 402653184 | bytes 2293760 | tf_op jit(solution)/shard_map/pallas_call | solution.py:31
  (84 shorter events, 15.0 us)
Async XLA Ops:
  6.6 50.9 %all-to-all-start = ((bf16[16,3,8,2048]{3,2,1,0:T(8,128)(2,1)}), bf16[16,3,8,2048]{3,2,1,0:T(8,128)(2,1)S(1)}, u32[]{:S(2)}, u32[]{:S(2)}) async-start(bf16[16,3,8,2048]{3,2,1,0:T(8,128)(2,1)} %shard_map.220), calls=%async_computation | async-start | bytes 3145728 | tf_op jit(solution)/shard_map/all_to_all | solution.py:396
  15.2 13.9 %collective-permute-start.1 = (bf16[128,2048]{1,0:T(8,128)(2,1)S(1)}, bf16[128,2048]{1,0:T(8,128)(2,1)S(1)}, u32[]{:S(2)}, u32[]{:S(2)}) collective-permute-start(bf16[128,2048]{1,0:T(8,128)(2,1)S(1)} %copy-done.12), channel_id=1, source_target_pairs={{0,2},{1,3},{2,4},{3,5},{4,6},{5,7},{6,0},{7,1},{8,10},{9,11},{10,... | collective-permute-start | bytes 1572872 | tf_op jit(solution)/shard_map/ppermute | solution.py:384
  16.6 14.3 %collective-permute-start.3 = (bf16[128,2048]{1,0:T(8,128)(2,1)S(1)}, bf16[128,2048]{1,0:T(8,128)(2,1)S(1)}, u32[]{:S(2)}, u32[]{:S(2)}) collective-permute-start(bf16[128,2048]{1,0:T(8,128)(2,1)S(1)} %copy-done.12), channel_id=1, source_target_pairs={{0,6},{1,7},{2,0},{3,1},{4,2},{5,3},{6,4},{7,5},{8,14},{9,15},{10,... | collective-permute-start | bytes 1572872 | tf_op jit(solution)/shard_map/ppermute | solution.py:384
  18.1 23.0 %collective-permute-start = (bf16[128,2048]{1,0:T(8,128)(2,1)S(1)}, bf16[128,2048]{1,0:T(8,128)(2,1)S(1)}, u32[]{:S(2)}, u32[]{:S(2)}) collective-permute-start(bf16[128,2048]{1,0:T(8,128)(2,1)S(1)} %copy-done.12), channel_id=1, source_target_pairs={{0,1},{1,0},{2,3},{3,2},{4,5},{5,4},{6,7},{7,6},{8,9},{9,8},{10,11... | collective-permute-start | bytes 1572872 | tf_op jit(solution)/shard_map/ppermute | solution.py:380
  29.1 13.7 %copy-start.17 = (bf16[128,2048]{1,0:T(8,128)(2,1)}, bf16[128,2048]{1,0:T(8,128)(2,1)S(1)}, u32[]{:S(2)}) copy-start(bf16[128,2048]{1,0:T(8,128)(2,1)S(1)} %collective-permute-done.1.refs_2_) | copy-start | bytes 1572868
  29.1 12.0 %collective-permute-start.2 = (bf16[128,2048]{1,0:T(8,128)(2,1)S(1)}, bf16[128,2048]{1,0:T(8,128)(2,1)S(1)}, u32[]{:S(2)}, u32[]{:S(2)}) collective-permute-start(bf16[128,2048]{1,0:T(8,128)(2,1)S(1)} %collective-permute-done.1.refs_2_), channel_id=1, source_target_pairs={{0,1},{1,0},{2,3},{3,2},{4,5},{5,4},{6,7},{7,6},{8,9},{9,8},{10,11... | collective-permute-start | bytes 1572872 | tf_op jit(solution)/shard_map/ppermute | solution.py:380
  30.9 11.9 %collective-permute-start.4 = (bf16[128,2048]{1,0:T(8,128)(2,1)S(1)}, bf16[128,2048]{1,0:T(8,128)(2,1)}, u32[]{:S(2)}, u32[]{:S(2)}) collective-permute-start(bf16[128,2048]{1,0:T(8,128)(2,1)S(1)} %collective-permute-done.3.refs_4_), channel_id=1, source_target_pairs={{0,1},{1,0},{2,3},{3,2},{4,5},{5,4},{6,7},{7,6},{8,9},{9,8},{10,11... | collective-permute-start | bytes 1572872 | tf_op jit(solution)/shard_map/ppermute | solution.py:380
  31.0 8.7 %collective-permute-start.5 = (bf16[64,2048]{1,0:T(8,128)(2,1)S(1)}, bf16[64,2048]{1,0:T(8,128)(2,1)S(1)}, u32[]{:S(2)}, u32[]{:S(2)}) collective-permute-start(bf16[64,2048]{1,0:T(8,128)(2,1)S(1)} %slice.8), channel_id=1, source_target_pairs={{0,2},{1,3},{2,4},{3,5},{4,6},{5,7},{6,0},{7,1},{8,10},{9,11},{10,... | collective-permute-start | bytes 786440 | tf_op jit(solution)/shard_map/ppermute | solution.py:384
  32.3 8.7 %collective-permute-start.6 = (bf16[64,2048]{1,0:T(8,128)(2,1)S(1)}, bf16[64,2048]{1,0:T(8,128)(2,1)S(1)}, u32[]{:S(2)}, u32[]{:S(2)}) collective-permute-start(bf16[64,2048]{1,0:T(8,128)(2,1)S(1)} %slice.9), channel_id=1, source_target_pairs={{0,6},{1,7},{2,0},{3,1},{4,2},{5,3},{6,4},{7,5},{8,14},{9,15},{10,... | collective-permute-start | bytes 786440 | tf_op jit(solution)/shard_map/ppermute | solution.py:384
  39.7 9.6 %collective-permute-start.7 = (bf16[64,2048]{1,0:T(8,128)(2,1)S(1)}, bf16[64,2048]{1,0:T(8,128)(2,1)S(1)}, u32[]{:S(2)}, u32[]{:S(2)}) collective-permute-start(bf16[64,2048]{1,0:T(8,128)(2,1)S(1)} %collective-permute-done.5.b0), channel_id=1, source_target_pairs={{0,1},{1,0},{2,3},{3,2},{4,5},{5,4},{6,7},{7,6},{8,9},{9,8},{10,11... | collective-permute-start | bytes 786440 | tf_op jit(solution)/shard_map/ppermute | solution.py:380
  41.0 8.4 %collective-permute-start.8 = (bf16[64,2048]{1,0:T(8,128)(2,1)S(1)}, bf16[64,2048]{1,0:T(8,128)(2,1)S(1)}, u32[]{:S(2)}, u32[]{:S(2)}) collective-permute-start(bf16[64,2048]{1,0:T(8,128)(2,1)S(1)} %collective-permute-done.6.b1), channel_id=1, source_target_pairs={{0,1},{1,0},{2,3},{3,2},{4,5},{5,4},{6,7},{7,6},{8,9},{9,8},{10,11... | collective-permute-start | bytes 786440 | tf_op jit(solution)/shard_map/ppermute | solution.py:380
  59.7 14.2 %copy-start.2 = (s32[2]{0:T(128)S(1)}, s32[2]{0:T(128)}, u32[]{:S(2)}) copy-start(s32[2]{0:T(128)} %pad_add_fusion.1.me_ref) | copy-start | bytes 28
  59.7 19.1 %copy-start.3 = (f32[1024,1]{0,1:T(1,128)S(1)}, f32[1024,1]{0,1:T(1,128)}, u32[]{:S(2)}) copy-start(f32[1024,1]{0,1:T(1,128)} %param.22) | copy-start | bytes 12292
  59.7 19.1 %copy-start.6 = (bf16[1024,256]{1,0:T(8,128)(2,1)S(1)}, bf16[1024,256]{1,0:T(8,128)(2,1)}, u32[]{:S(2)}) copy-start(bf16[1024,256]{1,0:T(8,128)(2,1)} %get-tuple-element.33.v_hbm) | copy-start | bytes 1572868
  59.7 19.1 %copy-start.10 = (bf16[1024,128]{1,0:T(8,128)(2,1)S(1)}, bf16[1024,128]{1,0:T(8,128)(2,1)}, u32[]{:S(2)}) copy-start(bf16[1024,128]{1,0:T(8,128)(2,1)} %get-tuple-element.31.q_hbm) | copy-start | bytes 786436
  59.7 19.1 %copy-start.11 = (bf16[1024,128]{1,0:T(8,128)(2,1)S(1)}, bf16[1024,128]{1,0:T(8,128)(2,1)}, u32[]{:S(2)}) copy-start(bf16[1024,128]{1,0:T(8,128)(2,1)} %get-tuple-element.32.k_hbm) | copy-start | bytes 786436
  59.7 22.8 %copy-start = (bf16[1024,256]{1,0:T(8,128)(2,1)S(1)}, bf16[1024,256]{1,0:T(8,128)(2,1)}, u32[]{:S(2)}) copy-start(bf16[1024,256]{1,0:T(8,128)(2,1)} %get-tuple-element.36.gate_ref) | copy-start | bytes 1572868
  59.7 22.8 %copy-start.4 = (f32[256]{0:T(256)S(1)}, f32[256]{0:T(256)}, u32[]{:S(2)}) copy-start(f32[256]{0:T(256)} %param.28) | copy-start | bytes 3076
  59.8 31.8 %all-to-all-start.1 = ((bf16[8,48,2048]{2,1,0:T(8,128)(2,1)}), bf16[8,48,2048]{2,1,0:T(8,128)(2,1)}, u32[]{:S(2)}, u32[]{:S(2)}) async-start(bf16[8,48,2048]{2,1,0:T(8,128)(2,1)} %bitcast.8), calls=%async_computation.1 | async-start | bytes 3145728 | tf_op jit(solution)/shard_map/all_to_all | solution.py:396
  64.5 21.8 %collective-permute-start.16 = (bf16[256,2048]{1,0:T(8,128)(2,1)S(1)}, bf16[256,2048]{1,0:T(8,128)(2,1)S(1)}, u32[]{:S(2)}, u32[]{:S(2)}) collective-permute-start(bf16[256,2048]{1,0:T(8,128)(2,1)S(1)} %copy-done.5), channel_id=1, source_target_pairs={{0,1},{1,0},{2,3},{3,2},{4,5},{5,4},{6,7},{7,6},{8,9},{9,8},{10,11... | collective-permute-start | bytes 3145736 | tf_op jit(solution)/shard_map/ppermute | solution.py:380
  64.7 3.9 %collective-permute-start.10 = (bf16[136,256]{1,0:T(8,128)(2,1)S(1)}, bf16[136,256]{1,0:T(8,128)(2,1)S(1)}, u32[]{:S(2)}, u32[]{:S(2)}) collective-permute-start(bf16[136,256]{1,0:T(8,128)(2,1)S(1)} %copy-done.1), channel_id=1, source_target_pairs={{0,24},{8,0},{16,8},{24,16},{32,56},{40,32},{48,40},{56,48},{64,88... | collective-permute-start | bytes 208904 | tf_op jit(solution)/shard_map/ppermute | solution.py:388
  67.3 5.1 %collective-permute-start.11 = (bf16[136,256]{1,0:T(8,128)(2,1)S(1)}, bf16[136,256]{1,0:T(8,128)(2,1)S(1)}, u32[]{:S(2)}, u32[]{:S(2)}) collective-permute-start(bf16[136,256]{1,0:T(8,128)(2,1)S(1)} %copy-done.1), channel_id=1, source_target_pairs={{0,16},{8,24},{16,0},{24,8},{32,48},{40,56},{48,32},{56,40},{64,80... | collective-permute-start | bytes 208904 | tf_op jit(solution)/shard_map/ppermute | solution.py:388
  67.8 6.1 %collective-permute-start.9 = (bf16[136,256]{1,0:T(8,128)(2,1)S(1)}, bf16[136,256]{1,0:T(8,128)(2,1)S(1)}, u32[]{:S(2)}, u32[]{:S(2)}) collective-permute-start(bf16[136,256]{1,0:T(8,128)(2,1)S(1)} %copy-done.1), channel_id=1, source_target_pairs={{0,8},{8,16},{16,24},{24,0},{32,40},{40,48},{48,56},{56,32},{64,72... | collective-permute-start | bytes 208904 | tf_op jit(solution)/shard_map/ppermute | solution.py:388
  74.6 6.1 %collective-permute-start.12 = (bf16[136,256]{1,0:T(8,128)(2,1)S(1)}, bf16[136,256]{1,0:T(8,128)(2,1)S(1)}, u32[]{:S(2)}, u32[]{:S(2)}) collective-permute-start(bf16[136,256]{1,0:T(8,128)(2,1)S(1)} %get-tuple-element.28.p0), channel_id=1, source_target_pairs={{0,32},{8,40},{16,48},{24,56},{32,64},{40,72},{48,80},{56,88},{64,... | collective-permute-start | bytes 208904 | tf_op jit(solution)/shard_map/ppermute | solution.py:392
  75.9 4.8 %collective-permute-start.13 = (bf16[136,256]{1,0:T(8,128)(2,1)S(1)}, bf16[136,256]{1,0:T(8,128)(2,1)S(1)}, u32[]{:S(2)}, u32[]{:S(2)}) collective-permute-start(bf16[136,256]{1,0:T(8,128)(2,1)S(1)} %get-tuple-element.28.p0), channel_id=1, source_target_pairs={{0,96},{8,104},{16,112},{24,120},{32,0},{40,8},{48,16},{56,24},{64... | collective-permute-start | bytes 208904 | tf_op jit(solution)/shard_map/ppermute | solution.py:392
  77.3 5.2 %collective-permute-start.14 = (bf16[136,256]{1,0:T(8,128)(2,1)S(1)}, bf16[136,256]{1,0:T(8,128)(2,1)S(1)}, u32[]{:S(2)}, u32[]{:S(2)}) collective-permute-start(bf16[136,256]{1,0:T(8,128)(2,1)S(1)} %get-tuple-element.28.p0), channel_id=1, source_target_pairs={{0,64},{8,72},{16,80},{24,88},{32,96},{40,104},{48,112},{56,120},{... | collective-permute-start | bytes 208904 | tf_op jit(solution)/shard_map/ppermute | solution.py:392
  84.0 3.4 %collective-permute-start.15 = (bf16[512,256]{1,0:T(8,128)(2,1)S(1)}, bf16[512,256]{1,0:T(8,128)(2,1)S(1)}, u32[]{:S(2)}, u32[]{:S(2)}) collective-permute-start(bf16[512,256]{1,0:T(8,128)(2,1)S(1)} %get-tuple-element.38), channel_id=1, source_target_pairs={{0,1},{1,0},{2,3},{3,2},{4,5},{5,4},{6,7},{7,6},{8,9},{9,8},{10,11... | collective-permute-start | bytes 786440 | tf_op jit(solution)/shard_map/ppermute | solution.py:380
  103.5 10.9 %copy-start.20 = (f32[128,2]{0,1:T(2,128)S(1)}, f32[128,2]{0,1:T(2,128)}, u32[]{:S(2)}) copy-start(f32[128,2]{0,1:T(2,128)} %param.34) | copy-start | bytes 3076
  103.5 56.4 %all-to-all-start.2 = ((bf16[128,3,2048]{2,1,0:T(4,128)(2,1)}), bf16[128,3,2048]{2,1,0:T(4,128)(2,1)S(1)}, u32[]{:S(2)}, u32[]{:S(2)}) async-start(bf16[128,3,2048]{2,1,0:T(4,128)(2,1)} %shard_map.222), calls=%async_computation.2 | async-start | bytes 4194304 | tf_op jit(solution)/shard_map/all_to_all | solution.py:396
  109.7 36.6 %collective-permute-start.17 = (bf16[128,2048]{1,0:T(8,128)(2,1)}, bf16[128,2048]{1,0:T(8,128)(2,1)S(1)}, u32[]{:S(2)}, u32[]{:S(2)}) collective-permute-start(bf16[128,2048]{1,0:T(8,128)(2,1)} %copy-done.9), channel_id=1, source_target_pairs={{0,2},{1,3},{2,4},{3,5},{4,6},{5,7},{6,0},{7,1},{8,10},{9,11},{10,... | collective-permute-start | bytes 1572872 | tf_op jit(solution)/shard_map/ppermute | solution.py:384
  111.1 35.2 %collective-permute-start.18 = (bf16[128,2048]{1,0:T(8,128)(2,1)}, bf16[128,2048]{1,0:T(8,128)(2,1)}, u32[]{:S(2)}, u32[]{:S(2)}) collective-permute-start(bf16[128,2048]{1,0:T(8,128)(2,1)} %copy-done.8), channel_id=1, source_target_pairs={{0,6},{1,7},{2,0},{3,1},{4,2},{5,3},{6,4},{7,5},{8,14},{9,15},{10,... | collective-permute-start | bytes 1572872 | tf_op jit(solution)/shard_map/ppermute | solution.py:384
  112.5 45.1 %collective-permute-start.19 = (bf16[128,2048]{1,0:T(8,128)(2,1)}, bf16[128,2048]{1,0:T(8,128)(2,1)}, u32[]{:S(2)}, u32[]{:S(2)}) collective-permute-start(bf16[128,2048]{1,0:T(8,128)(2,1)} %copy-done.7), channel_id=1, source_target_pairs={{0,4},{1,5},{2,6},{3,7},{4,0},{5,1},{6,2},{7,3},{8,12},{9,13},{10,... | collective-permute-start | bytes 1572872 | tf_op jit(solution)/shard_map/ppermute | solution.py:384
  (15 other events, 73.4 us)
